TPU v7x, 512 devices: a 8x2x16 block of a 8x16x16 slice. The times are simulated.
512 devices in a mesh: grp: 2 (over y), kv: 16 (over z), tp: 16 (over x, core).
Axes of the slice: x: 8, y: 2, z: 16, core: 2. Of those that a mesh axis runs over, the one named last changes fastest.
The devices are a block of a 8x16x16 slice.
Arguments:
- tokens: bfloat16 [640, 4096], P('grp', ('kv', 'tp')), parts along dimension 0, may hold values from -65 to 65
- lengths: int32 [640], P(('grp', 'kv')), parts along dimension 0, may hold values from 1 to 16384, 1310720 in all
- memory: float32 [640, 16, 128, 128], P(('grp', 'kv'), 'tp'), parts along dimension 0, may hold values from -6 to 6
- norm_attn: bfloat16 [4096], P('kv'), may hold values from 0.099609375 to 1.8984375
- w_query: bfloat16 [4096, 2048], P('kv', 'tp'), may hold values from -0.09375 to 0.09375
- w_key: bfloat16 [4096, 2048], P('kv', 'tp'), may hold values from -0.09375 to 0.09375
- w_value: bfloat16 [4096, 2048], P('kv', 'tp'), may hold values from -0.09375 to 0.09375
- w_gate: bfloat16 [4096, 2048], P('kv', 'tp'), may hold values from -0.09375 to 0.09375
- head_gain: bfloat16 [2048], P('tp'), may hold values from 0.099609375 to 1.8984375
- w_out: bfloat16 [2048, 4096], P('tp', 'kv'), may hold values from -0.1875 to 0.1875
- norm_mlp: bfloat16 [4096], P('kv'), may hold values from 0.099609375 to 1.8984375
- w_gate_mlp: bfloat16 [4096, 14336], P('kv', 'tp'), may hold values from -0.09375 to 0.09375
- w_up: bfloat16 [4096, 14336], P('kv', 'tp'), may hold values from -0.09375 to 0.09375
- w_down: bfloat16 [14336, 4096], P('tp', 'kv'), may hold values from -0.0625 to 0.0625
Outputs:
- result: bfloat16 [640, 4096], P('grp', ('kv', 'tp')), parts along dimension 0
- new_memory: float32 [640, 16, 128, 128], P(('grp', 'kv'), 'tp'), parts along dimension 0
There are 2 independent parts, one for each index of `grp`. A program takes and returns all parts, laid end to end along the dimension named above; an argument that names none is the same for every part. Nothing has to cross between parts.
Inputs may be any that keep to these rules, and one draw needn't show every extreme that they name: Within each part along grp the lengths sum to 1310720 and the longest is exactly 16384.
All inputs are finite; a program needn't handle non-finite values. No bound on the sum of `lengths` on one device may be relied on, other than what follows from the above.
Results may differ from a plain program's by a relative error of at most 0.025.
Values may be sent and summed in bfloat16 or wider, within the bound.
No kernel may reach another device: no remote copies, remote signals or barrier semaphores. Data moves between devices by JAX's collectives and lax.ppermute only.
A program may use at most 64 MiB of HBM per device.

v0:
```python
import jax
import jax.numpy as jnp
from jax import lax
from jax.sharding import PartitionSpec as P

D = 4096
HEADS = 16


epsilon = 1e-06


def from_everyone(array, axis):
    copies = jnp.broadcast_to(array, (lax.axis_size(axis), *array.shape))
    return lax.all_to_all(copies, axis, split_axis=0, concat_axis=0, tiled=True)


def taken_together(array, axis):
    everything = from_everyone(array, axis)
    return jnp.sum(everything, axis=0)


def in_blocks(array, dim, size):
    lengths = array.shape
    pieces = array.reshape(*lengths[:dim], size, lengths[dim] // size, *lengths[dim + 1 :])
    return jnp.moveaxis(pieces, dim, 0)


def sum_at_owner(array, axis, dim):
    size = lax.axis_size(axis)
    pieces = lax.all_to_all(in_blocks(array, dim, size), axis, 0, 0, tiled=True)
    return jnp.sum(pieces.astype(jnp.float32), axis=0)


def rotate(values, position):
    half_width = values.shape[-1] // 2
    inverse = 10000.0 ** (-jnp.arange(half_width, dtype=jnp.float32) / half_width)
    angles = position[:, None] * inverse[None, :]
    cosine = jnp.cos(angles)[:, None, :]
    sine = jnp.sin(angles)[:, None, :]
    first = values[..., :half_width]
    second = values[..., half_width:]
    return jnp.concatenate(
        [first * cosine - second * sine, second * cosine + first * sine], axis=-1
    )


def head_decay(head_index):
    exponent = -5.0 - head_index.astype(jnp.float32) * (7.0 / max(HEADS - 1, 1))
    return 1.0 - jnp.exp2(exponent)


def retain(memory, queries, key_rows, value_rows, gate_rows, head_gain, decay_rate):
    new_memory = (
        decay_rate[None, :, None, None] * memory
        + key_rows[:, :, :, None] * value_rows[:, :, None, :]
    )
    readout = jnp.einsum(
        "bhd,bhde->bhe",
        queries * queries.shape[-1] ** (-0.5),
        new_memory,
        precision=lax.Precision.HIGHEST,
    )
    centred = readout - jnp.mean(readout, axis=-1, keepdims=True)
    normed = centred * lax.rsqrt(jnp.mean(centred * centred, axis=-1, keepdims=True) + epsilon)
    normed = normed.reshape(readout.shape[0], -1) * head_gain.astype(jnp.float32)
    return (new_memory, (normed * jax.nn.silu(gate_rows)).astype(jnp.bfloat16))


def per_device(
    tokens,
    lengths,
    memory,
    norm_attn,
    w_query,
    w_key,
    w_value,
    w_gate,
    head_gain,
    w_out,
    norm_mlp,
    w_gate_mlp,
    w_up,
    w_down,
):
    own_count = memory.shape[0]
    heads_local = memory.shape[1]
    head_size = memory.shape[2]
    width_local = w_query.shape[1]
    gathered = lax.all_gather(tokens, "tp", axis=1, tiled=True)
    tok_float = gathered.astype(jnp.float32)
    square_part = jnp.sum(tok_float * tok_float, axis=1)
    scaled = (tok_float * norm_attn.astype(jnp.float32)).astype(jnp.bfloat16)
    own_start = lax.axis_index("kv") * own_count
    square_total = taken_together(square_part, "kv")
    own_squares = lax.dynamic_slice_in_dim(square_total, own_start, own_count, 0)
    block_rows = scaled
    projected = sum_at_owner(
        jnp.concatenate(
            [
                jnp.dot(block_rows, weight, preferred_element_type=jnp.float32)
                for weight in (w_query, w_key, w_value, w_gate)
            ],
            axis=1,
        ).astype(jnp.bfloat16),
        "kv",
        0,
    )
    projected = projected * lax.rsqrt(own_squares / D + epsilon)[:, None]
    position = lengths.astype(jnp.float32)
    queries = rotate(
        projected[:, :width_local].reshape(own_count, heads_local, head_size), position
    )
    key_rows = rotate(
        projected[:, width_local : 2 * width_local].reshape(own_count, heads_local, head_size),
        position,
    )
    value_rows = projected[:, 2 * width_local : 3 * width_local].reshape(
        own_count, heads_local, head_size
    )
    gate_rows = projected[:, 3 * width_local :]
    decay_rate = head_decay(lax.axis_index("tp") * heads_local + jnp.arange(heads_local))
    new_memory, mixed = retain(
        memory, queries, key_rows, value_rows, gate_rows, head_gain, decay_rate
    )
    attn_part = jnp.dot(
        lax.all_gather(mixed, "kv", axis=0, tiled=True), w_out, preferred_element_type=jnp.float32
    )
    attn_total = sum_at_owner(attn_part.astype(jnp.bfloat16), "tp", 1)
    middle = (tokens.astype(jnp.float32) + attn_total).astype(jnp.bfloat16)
    mid_float = middle.astype(jnp.float32)
    gathered_mid = lax.all_gather(middle, "tp", axis=1, tiled=True)
    gathered_float = gathered_mid.astype(jnp.float32)
    mid_squares = jnp.sum(gathered_float * gathered_float, axis=1)
    scaled_mid = (gathered_float * norm_mlp.astype(jnp.float32)).astype(jnp.bfloat16)
    ff_local = w_up.shape[1]
    pieces = 1
    span = scaled_mid.shape[0] // pieces
    own_span = span // lax.axis_size("kv")
    span_start = lax.axis_index("kv") * own_span
    square_sums = taken_together(mid_squares, "kv")
    span_squares = lax.dynamic_slice_in_dim(square_sums, span_start, own_span, 0)
    block_rows = scaled_mid
    both_terms = lax.psum_scatter(
        jnp.concatenate(
            [
                jnp.dot(block_rows, w_gate_mlp, preferred_element_type=jnp.float32),
                jnp.dot(block_rows, w_up, preferred_element_type=jnp.float32),
            ],
            axis=1,
        ).astype(jnp.bfloat16),
        "kv",
        scatter_dimension=0,
        tiled=True,
    ).astype(jnp.float32)
    inv_mlp = lax.rsqrt(span_squares / D + epsilon)[:, None]
    gate_mlp = inv_mlp * both_terms[:, :ff_local]
    up_rows = inv_mlp * both_terms[:, ff_local:]
    hidden = (jax.nn.silu(gate_mlp) * up_rows).astype(jnp.bfloat16)
    partial_mlp = jnp.dot(
        lax.all_gather(hidden, "kv", axis=0, tiled=True), w_down, preferred_element_type=jnp.float32
    )
    results = sum_at_owner(partial_mlp.astype(jnp.bfloat16), "tp", 1)
    return ((mid_float + results).astype(jnp.bfloat16), new_memory)


def solution(mesh):
    in_specs = (
        P("grp", ("kv", "tp")),
        P(("grp", "kv")),
        P(("grp", "kv"), "tp", None, None),
        P("kv"),
        P("kv", "tp"),
        P("kv", "tp"),
        P("kv", "tp"),
        P("kv", "tp"),
        P("tp"),
        P("tp", "kv"),
        P("kv"),
        P("kv", "tp"),
        P("kv", "tp"),
        P("tp", "kv"),
    )
    out_specs = (P("grp", ("kv", "tp")), P(("grp", "kv"), "tp", None, None))
    return jax.shard_map(
        per_device, mesh=mesh, in_specs=in_specs, out_specs=out_specs, check_vma=False
    )
```

profile of v0, /device:TPU:65, one launch (start us, length us, event | category | flops | bytes accessed | tf_op | source)
XLA Modules:
  0.0 281.9 jit_solution(7506747860716999850)
XLA Ops:
  0.7 56.5 %all_gather.12 = bf16[320,256]{0,1:T(8,128)(2,1)S(1)} all-gather(bf16[320,16]{0,1:T(8,128)(2,1)} %param.14), channel_id=1, replica_groups=mesh['grp'=2,'kv'=16,'tp'=16] {'tp'}, dimensions={1}, use_global_device_ids=true | all-gather | bytes 174080 | tf_op jit(solution)/shard_map/all_gather | solution.py:90
  57.2 0.6 broadcast_in_dim.4
  57.8 7.1 %all-to-all-start.1 = ((f32[16,1,320]{2,1,0:T(1,128)}), f32[16,1,320]{2,1,0:T(1,128)S(1)}, u32[]{:S(2)}, u32[]{:S(2)}) async-start(f32[16,1,320]{2,1,0:T(1,128)} %broadcast_in_dim.4), calls=%async_computation.1 | async-start | bytes 49152 | tf_op jit(solution)/shard_map/all_to_all | solution.py:15
  64.9 0.7 convert_element_type.69
  65.6 1.1 convolution_convert_fusion.6
  66.8 1.2 convolution_convert_fusion.5
  68.7 0.8 pad_maximum_fusion.1
  69.5 6.7 %all-to-all-done.1 = f32[16,1,320]{2,1,0:T(1,128)S(1)} async-done(((f32[16,1,320]{2,1,0:T(1,128)}), f32[16,1,320]{2,1,0:T(1,128)S(1)}, u32[]{:S(2)}, u32[]{:S(2)}) %all-to-all-start.1) | async-done | bytes 20512 | tf_op jit(solution)/shard_map/all_to_all | solution.py:15
  76.2 4.7 %all-to-all-start = ((bf16[16,20,512]{2,1,0:T(8,128)(2,1)}), bf16[16,20,512]{2,1,0:T(8,128)(2,1)S(1)}, u32[]{:S(2)}, u32[]{:S(2)}) async-start(bf16[16,20,512]{2,1,0:T(8,128)(2,1)} %pad_maximum_fusion.1), calls=%async_computation | async-start | bytes 786432 | tf_op jit(solution)/shard_map/all_to_all | solution.py:31
  81.2 17.7 %all-to-all-done = bf16[16,20,512]{2,1,0:T(8,128)(2,1)S(1)} async-done(((bf16[16,20,512]{2,1,0:T(8,128)(2,1)}), bf16[16,20,512]{2,1,0:T(8,128)(2,1)S(1)}, u32[]{:S(2)}, u32[]{:S(2)}) %all-to-all-start) | async-done | bytes 327712 | tf_op jit(solution)/shard_map/all_to_all | solution.py:31
  99.3 0.4 multiply_add_fusion
  99.8 1.2 fusion.1
  101.4 26.0 %all-gather = bf16[16,20,128]{2,1,0:T(8,128)(2,1)S(1)} all-gather(bf16[1,20,128]{2,1,0:T(8,128)(2,1)S(1)} %fusion.28), channel_id=1, replica_groups=mesh['grp'=2,'kv'=16,'tp'=16] {'kv'}, dimensions={0}, use_global_device_ids=true | all-gather | bytes 87040 | tf_op jit(solution)/shard_map/all_gather | solution.py:127
  127.6 0.8 copy.23
  128.4 15.3 %all-to-all-start.2 = ((bf16[16,320,16]{1,2,0:T(8,128)(2,1)}), bf16[16,320,16]{1,2,0:T(8,128)(2,1)S(1)}, u32[]{:S(2)}, u32[]{:S(2)}) async-start(bf16[16,320,16]{1,2,0:T(8,128)(2,1)} %bitcast.10), calls=%async_computation.2 | async-start | bytes 393216 | tf_op jit(solution)/shard_map/all_to_all | solution.py:31
  143.7 1.3 dynamic-slice.4
  145.7 8.3 %all-to-all-done.2 = bf16[16,320,16]{1,2,0:T(8,128)(2,1)S(1)} async-done(((bf16[16,320,16]{1,2,0:T(8,128)(2,1)}), bf16[16,320,16]{1,2,0:T(8,128)(2,1)S(1)}, u32[]{:S(2)}, u32[]{:S(2)}) %all-to-all-start.2) | async-done | bytes 163872 | tf_op jit(solution)/shard_map/all_to_all | solution.py:31
  154.0 15.1 %all_gather.14 = bf16[320,256]{0,1:T(8,128)(2,1)S(1)} all-gather(bf16[320,16]{0,1:T(8,128)(2,1)S(1)} %add_convert_fusion.1), channel_id=1, replica_groups=mesh['grp'=2,'kv'=16,'tp'=16] {'tp'}, dimensions={1}, use_global_device_ids=true | all-gather | bytes 174080 | tf_op jit(solution)/shard_map/all_gather | solution.py:132
  169.1 0.6 broadcast_in_dim.5
  169.8 4.7 %all-to-all-start.3 = ((f32[16,1,320]{2,1,0:T(1,128)}), f32[16,1,320]{2,1,0:T(1,128)S(1)}, u32[]{:S(2)}, u32[]{:S(2)}) async-start(f32[16,1,320]{2,1,0:T(1,128)} %broadcast_in_dim.5), calls=%async_computation.3 | async-start | bytes 49152 | tf_op jit(solution)/shard_map/all_to_all | solution.py:15
  174.4 0.4 convolution_convert_fusion
  174.9 0.4 convolution_convert_fusion.1
  175.4 32.2 %fusion = bf16[24,1792]{1,0:T(8,128)(2,1)S(1)} fusion(bf16[320,1792]{1,0:T(8,128)(2,1)S(1)} %pad_maximum_fusion), kind=kCustom, calls=%all-reduce-scatter | all-reduce-scatter fusion | flops 688129 | bytes 1234944
  207.6 2.7 collective-permute-start.1
  210.3 2.9 %collective-permute-start = (bf16[24,1792]{1,0:T(8,128)(2,1)S(1)}, bf16[24,1792]{1,0:T(8,128)(2,1)S(1)}, u32[]{:S(2)}, u32[]{:S(2)}) collective-permute-start(bf16[24,1792]{1,0:T(8,128)(2,1)S(1)} %fusion), channel_id=1, source_target_pairs={{0,16},{16,32},{32,48},{48,64},{64,80},{80,96},{96,112},{112,128},... | collective-permute-start | bytes 258056
  213.3 5.5 %collective-permute-start.2 = (bf16[12,1792]{1,0:T(8,128)(2,1)S(1)}, bf16[12,1792]{1,0:T(8,128)(2,1)S(1)}, u32[]{:S(2)}, u32[]{:S(2)}) collective-permute-start(bf16[12,1792]{1,0:T(8,128)(2,1)S(1)} %slice.50), channel_id=1, source_target_pairs={{0,48},{16,64},{32,80},{48,96},{64,112},{80,128},{96,144},{112,160... | collective-permute-start | bytes 129032
  218.9 1.1 collective-permute-done.2
  220.1 0.6 concatenate.40
  220.8 28.5 %all-gather.1 = bf16[16,20,896]{2,1,0:T(8,128)(2,1)S(1)} all-gather(bf16[1,20,896]{2,1,0:T(8,128)(2,1)S(1)} %fusion.11), channel_id=1, replica_groups=mesh['grp'=2,'kv'=16,'tp'=16] {'kv'}, dimensions={0}, use_global_device_ids=true | all-gather | bytes 609280 | tf_op jit(solution)/shard_map/all_gather | solution.py:161
  249.5 0.3 convolution_convert_fusion.2
  250.0 31.3 %all_to_all.27 = bf16[16,320,16]{1,2,0:T(8,128)(2,1)S(1)} all-to-all(bf16[16,320,16]{1,2,0:T(8,128)(2,1)S(1)} %bitcast.47), channel_id=1, replica_groups=mesh['grp'=2,'kv'=16,'tp'=16] {'tp'}, dimensions={0} | all-to-all | bytes 327680 | tf_op jit(solution)/shard_map/all_to_all | solution.py:31
  281.3 0.6 add_convert_fusion
  (65 shorter events, 2.8 us)
Async XLA Ops:
  0.6 173.8 %copy-start = (bf16[256,896]{1,0:T(8,128)(2,1)S(1)}, bf16[256,896]{1,0:T(8,128)(2,1)}, u32[]{:S(2)}) copy-start(bf16[256,896]{1,0:T(8,128)(2,1)} %param.26) | copy-start | bytes 1376260
  0.6 67.3 %copy-start.6 = (bf16[256,128]{1,0:T(8,128)(2,1)S(1)}, bf16[256,128]{1,0:T(8,128)(2,1)}, u32[]{:S(2)}) copy-start(bf16[256,128]{1,0:T(8,128)(2,1)} %param.21) | copy-start | bytes 196612
  0.7 67.7 %copy-start.7 = (bf16[256,128]{1,0:T(8,128)(2,1)S(1)}, bf16[256,128]{1,0:T(8,128)(2,1)}, u32[]{:S(2)}) copy-start(bf16[256,128]{1,0:T(8,128)(2,1)} %param.18) | copy-start | bytes 196612
  57.8 18.4 %all-to-all-start.1 = ((f32[16,1,320]{2,1,0:T(1,128)}), f32[16,1,320]{2,1,0:T(1,128)S(1)}, u32[]{:S(2)}, u32[]{:S(2)}) async-start(f32[16,1,320]{2,1,0:T(1,128)} %broadcast_in_dim.4), calls=%async_computation.1 | async-start | bytes 49152 | tf_op jit(solution)/shard_map/all_to_all | solution.py:15
  68.0 13.1 %copy-start.9 = (s32[20]{0:T(128)S(1)}, s32[20]{0:T(128)}, u32[]{:S(2)}) copy-start(s32[20]{0:T(128)} %param.15) | copy-start | bytes 244
  68.0 13.1 %copy-start.10 = (bf16[128]{0:T(256)(128)(2,1)S(1)}, bf16[128]{0:T(256)(128)(2,1)}, u32[]{:S(2)}) copy-start(bf16[128]{0:T(256)(128)(2,1)} %param.22) | copy-start | bytes 772
  68.7 30.7 %copy-start.2 = (f32[20,1,128,128]{3,2,1,0:T(8,128)S(1)}, f32[20,1,128,128]{3,2,1,0:T(8,128)}, u32[]{:S(2)}) copy-start(f32[20,1,128,128]{3,2,1,0:T(8,128)} %param.16) | copy-start | bytes 3932164
  76.2 22.7 %all-to-all-start = ((bf16[16,20,512]{2,1,0:T(8,128)(2,1)}), bf16[16,20,512]{2,1,0:T(8,128)(2,1)S(1)}, u32[]{:S(2)}, u32[]{:S(2)}) async-start(bf16[16,20,512]{2,1,0:T(8,128)(2,1)} %pad_maximum_fusion.1), calls=%async_computation | async-start | bytes 786432 | tf_op jit(solution)/shard_map/all_to_all | solution.py:31
  99.8 28.7 %copy-start.1 = (f32[20,1,128,128]{3,2,1,0:T(8,128)}, f32[20,1,128,128]{3,2,1,0:T(8,128)S(1)}, u32[]{:S(2)}) copy-start(f32[20,1,128,128]{3,2,1,0:T(8,128)S(1)} %multiply_add_fusion) | copy-start | bytes 3932164
  99.8 27.6 %copy-start.5 = (bf16[128,256]{1,0:T(8,128)(2,1)S(1)}, bf16[128,256]{1,0:T(8,128)(2,1)}, u32[]{:S(2)}) copy-start(bf16[128,256]{1,0:T(8,128)(2,1)} %param.23) | copy-start | bytes 196612
  99.8 43.9 %copy-start.11 = (bf16[256]{0:T(256)(128)(2,1)S(1)}, bf16[256]{0:T(256)(128)(2,1)}, u32[]{:S(2)}) copy-start(bf16[256]{0:T(256)(128)(2,1)} %param.24) | copy-start | bytes 1540
  99.8 54.2 %copy-start.8 = (bf16[320,16]{0,1:T(8,128)(2,1)S(1)}, bf16[320,16]{0,1:T(8,128)(2,1)}, u32[]{:S(2)}) copy-start(bf16[320,16]{0,1:T(8,128)(2,1)} %param.14) | copy-start | bytes 30724
  127.6 47.3 %copy-start.3 = (bf16[256,896]{1,0:T(8,128)(2,1)S(1)}, bf16[256,896]{1,0:T(8,128)(2,1)}, u32[]{:S(2)}) copy-start(bf16[256,896]{1,0:T(8,128)(2,1)} %param.25) | copy-start | bytes 1376260
  128.4 25.5 %all-to-all-start.2 = ((bf16[16,320,16]{1,2,0:T(8,128)(2,1)}), bf16[16,320,16]{1,2,0:T(8,128)(2,1)S(1)}, u32[]{:S(2)}, u32[]{:S(2)}) async-start(bf16[16,320,16]{1,2,0:T(8,128)(2,1)} %bitcast.10), calls=%async_computation.2 | async-start | bytes 393216 | tf_op jit(solution)/shard_map/all_to_all | solution.py:31
  169.8 49.1 %all-to-all-start.3 = ((f32[16,1,320]{2,1,0:T(1,128)}), f32[16,1,320]{2,1,0:T(1,128)S(1)}, u32[]{:S(2)}, u32[]{:S(2)}) async-start(f32[16,1,320]{2,1,0:T(1,128)} %broadcast_in_dim.5), calls=%async_computation.3 | async-start | bytes 49152 | tf_op jit(solution)/shard_map/all_to_all | solution.py:15
  207.6 12.4 %collective-permute-start.1 = (bf16[24,1792]{1,0:T(8,128)(2,1)S(1)}, bf16[24,1792]{1,0:T(8,128)(2,1)S(1)}, u32[]{:S(2)}, u32[]{:S(2)}) collective-permute-start(bf16[24,1792]{1,0:T(8,128)(2,1)S(1)} %fusion), channel_id=1, source_target_pairs={{0,32},{16,48},{32,64},{48,80},{64,96},{80,112},{96,128},{112,144}... | collective-permute-start | bytes 258056
  210.3 9.7 %collective-permute-start = (bf16[24,1792]{1,0:T(8,128)(2,1)S(1)}, bf16[24,1792]{1,0:T(8,128)(2,1)S(1)}, u32[]{:S(2)}, u32[]{:S(2)}) collective-permute-start(bf16[24,1792]{1,0:T(8,128)(2,1)S(1)} %fusion), channel_id=1, source_target_pairs={{0,16},{16,32},{32,48},{48,64},{64,80},{80,96},{96,112},{112,128},... | collective-permute-start | bytes 258056
  213.3 6.8 %collective-permute-start.2 = (bf16[12,1792]{1,0:T(8,128)(2,1)S(1)}, bf16[12,1792]{1,0:T(8,128)(2,1)S(1)}, u32[]{:S(2)}, u32[]{:S(2)}) collective-permute-start(bf16[12,1792]{1,0:T(8,128)(2,1)S(1)} %slice.50), channel_id=1, source_target_pairs={{0,48},{16,64},{32,80},{48,96},{64,112},{80,128},{96,144},{112,160... | collective-permute-start | bytes 129032
  220.6 28.8 %copy-start.4 = (bf16[896,256]{1,0:T(8,128)(2,1)S(1)}, bf16[896,256]{1,0:T(8,128)(2,1)}, u32[]{:S(2)}) copy-start(bf16[896,256]{1,0:T(8,128)(2,1)} %param.27) | copy-start | bytes 1376260
where the time goes:
time: 283 us; the launch traced here: 282 us
  blocking collectives  190 us (67%)
  starting transfers between devices  42.9 us (15%)
  waiting for transfers between devices  33.8 us (12%)
  matrix products  5.51 us (2%)
  local copies, waits for them, and re-layouts  4.37 us (2%)
  other arithmetic  4 us (1%)
    all_gather x1, blocking collectives, per_device(): gathered = lax.all_gather(tokens, 'tp', axis=1, tiled=True)  56.5 us
    unnamed x1, blocking collectives  32.2 us
    all_to_all x1, blocking collectives, sum_at_owner(): pieces = lax.all_to_all(in_blocks(array, dim, size), axis, 0, 0, tiled=True)  31.3 us
    all_gather x1, blocking collectives, per_device(): lax.all_gather(hidden, 'kv', axis=0, tiled=True)  28.5 us
    all_gather x1, blocking collectives, per_device(): lax.all_gather(mixed, 'kv', axis=0, tiled=True)  26 us
    all_to_all x2, waiting for transfers between devices, sum_at_owner(): pieces = lax.all_to_all(in_blocks(array, dim, size), axis, 0, 0, tiled=True)  25.9 us
    all_to_all x2, starting transfers between devices, sum_at_owner(): pieces = lax.all_to_all(in_blocks(array, dim, size), axis, 0, 0, tiled=True)  20 us
    all_gather x1, blocking collectives, per_device(): gathered_mid = lax.all_gather(middle, 'tp', axis=1, tiled=True)  15.1 us
  transfers between devices with their start and end apart: 7, of which 4 were waited for; matrix products, arithmetic and copies ran while one was open for 14% of the time, Pallas kernels for 0%

commit v1 on v0

v1 whole, which is shorter than its diff:
```python
import jax
import jax.numpy as jnp
from jax import lax
from jax.sharding import PartitionSpec as P


D = 4096
HEADS = 16


epsilon = 1e-06


def from_everyone(array, axis):
    copies = jnp.broadcast_to(array, (lax.axis_size(axis), *array.shape))
    return lax.all_to_all(copies, axis, split_axis=0, concat_axis=0, tiled=True)


def in_three(values):
    high = values.astype(jnp.bfloat16)
    rest = values - high.astype(jnp.float32)
    mid = rest.astype(jnp.bfloat16)
    low = (rest - mid.astype(jnp.float32)).astype(jnp.bfloat16)
    return high, mid, low


def rotate(values, cosine, sine):
    half_width = values.shape[-1] // 2
    first = values[..., :half_width]
    second = values[..., half_width:]
    return jnp.concatenate(
        [first * cosine - second * sine, second * cosine + first * sine], axis=-1
    )


def head_decay(head_index):
    exponent = -5.0 - head_index.astype(jnp.float32) * (7.0 / max(HEADS - 1, 1))
    return 1.0 - jnp.exp2(exponent)


def retain(memory, queries, key_rows, value_rows, gate_rows, head_gain, decay_rate):
    new_memory = (
        decay_rate[None, :, None, None] * memory
        + key_rows[:, :, :, None] * value_rows[:, :, None, :]
    )
    readout = jnp.einsum(
        "bhd,bhde->bhe",
        queries * queries.shape[-1] ** (-0.5),
        new_memory,
        precision=lax.Precision.HIGHEST,
    )
    centred = readout - jnp.mean(readout, axis=-1, keepdims=True)
    normed = centred * lax.rsqrt(jnp.mean(centred * centred, axis=-1, keepdims=True) + epsilon)
    normed = normed.reshape(readout.shape[0], -1) * head_gain.astype(jnp.float32)
    return (new_memory, (normed * jax.nn.silu(gate_rows)).astype(jnp.bfloat16))


def per_device(
    tokens,
    lengths,
    memory,
    norm_attn,
    w_query,
    w_key,
    w_value,
    w_gate,
    head_gain,
    w_out,
    norm_mlp,
    w_gate_mlp,
    w_up,
    w_down,
):
    f32, bf16 = jnp.float32, jnp.bfloat16
    n_kv, n_tp = lax.axis_size("kv"), lax.axis_size("tp")
    kv = lax.axis_index("kv")
    rows = tokens.shape[0]
    own = memory.shape[0]
    heads_local = memory.shape[1]
    head_size = memory.shape[2]
    width = w_query.shape[1]
    block = w_query.shape[0]
    ff = w_up.shape[1]

    tok = tokens.T
    gathered = from_everyone(tok, "tp").reshape(block, rows).astype(f32)
    squares = jnp.sum(gathered * gathered, axis=0)
    scaled = (gathered * norm_attn.astype(f32)[:, None]).astype(bf16)
    parts = jnp.concatenate(
        [
            lax.dot_general(scaled, w, (((0,), (0,)), ((), ())), preferred_element_type=f32)
            for w in (w_query, w_key, w_value, w_gate)
        ],
        axis=1,
    ).astype(bf16)
    terms = jnp.stack([t.reshape(n_kv, own) for t in in_three(squares)], axis=1)
    terms = jnp.pad(terms, ((0, 0), (0, 1), (0, parts.shape[1] - own)))
    sent = jnp.concatenate([parts.reshape(n_kv, own, -1), terms], axis=1)
    got = lax.all_to_all(sent, "kv", 0, 0, tiled=True)
    summed = jnp.sum(got.astype(f32), axis=0)
    own_squares = summed[own, :own] + summed[own + 1, :own] + summed[own + 2, :own]
    projected = summed[:own] * lax.rsqrt(own_squares / D + epsilon)[:, None]

    half = head_size // 2
    inverse = 10000.0 ** (-jnp.arange(half, dtype=f32) / half)
    angles = lengths.astype(f32)[:, None] * inverse[None, :]
    cosine, sine = jnp.cos(angles)[:, None, :], jnp.sin(angles)[:, None, :]
    heads = [
        projected[:, i * width : (i + 1) * width].reshape(own, heads_local, head_size)
        for i in range(3)
    ]
    decay_rate = head_decay(lax.axis_index("tp") * heads_local + jnp.arange(heads_local))
    new_memory, mixed = retain(
        memory,
        rotate(heads[0], cosine, sine),
        rotate(heads[1], cosine, sine),
        heads[2],
        projected[:, 3 * width :],
        head_gain,
        decay_rate,
    )

    mixed_all = from_everyone(mixed, "kv").reshape(rows, width)
    attn_part = lax.dot_general(
        w_out, mixed_all, (((0,), (1,)), ((), ())), preferred_element_type=f32
    ).astype(bf16)
    attn = lax.all_to_all(attn_part.reshape(n_tp, -1, rows), "tp", 0, 0, tiled=True)
    middle = (tok.astype(f32) + jnp.sum(attn.astype(f32), axis=0)).astype(bf16)

    mid_all = from_everyone(middle, "tp").reshape(block, rows).astype(f32)
    mid_squares = from_everyone(jnp.sum(mid_all * mid_all, axis=0)[None], "kv")
    scaled_mid = (mid_all * norm_mlp.astype(f32)[:, None]).astype(bf16)
    lanes = 128
    cuts = ff // lanes
    both = jnp.concatenate(
        [w_gate_mlp.reshape(block, cuts, lanes), w_up.reshape(block, cuts, lanes)], axis=2
    ).transpose(1, 0, 2)
    terms = jnp.concatenate(
        [
            lax.dot_general(scaled_mid, both[c], (((0,), (0,)), ((), ())), preferred_element_type=f32)
            for c in range(cuts)
        ],
        axis=0,
    ).astype(bf16)
    terms = lax.psum_scatter(terms, "kv", scatter_dimension=0, tiled=True)
    terms = terms.astype(f32)
    share = terms.shape[0]
    totals = jnp.sum(mid_squares, axis=(0, 1))
    inv_mlp = lax.rsqrt(totals / D + epsilon)
    inv_mlp = lax.dynamic_slice_in_dim(
        jnp.concatenate([inv_mlp, inv_mlp]), lax.rem(kv * share, rows), share, 0
    )[:, None]
    hidden = (jax.nn.silu(inv_mlp * terms[:, :lanes]) * (inv_mlp * terms[:, lanes:])).astype(bf16)
    hidden = lax.all_gather(hidden, "kv", axis=0, tiled=True).reshape(cuts, rows, lanes)
    down = lax.dot_general(
        w_down,
        hidden.transpose(1, 0, 2).reshape(rows, ff),
        (((0,), (1,)), ((), ())),
        preferred_element_type=f32,
    ).astype(bf16)
    down = lax.all_to_all(down.reshape(n_tp, -1, rows), "tp", 0, 0, tiled=True)
    result = (middle.astype(f32) + jnp.sum(down.astype(f32), axis=0)).astype(bf16)
    return (result.T, new_memory)


def solution(mesh):
    in_specs = (
        P("grp", ("kv", "tp")),
        P(("grp", "kv")),
        P(("grp", "kv"), "tp", None, None),
        P("kv"),
        P("kv", "tp"),
        P("kv", "tp"),
        P("kv", "tp"),
        P("kv", "tp"),
        P("tp"),
        P("tp", "kv"),
        P("kv"),
        P("kv", "tp"),
        P("kv", "tp"),
        P("tp", "kv"),
    )
    out_specs = (P("grp", ("kv", "tp")), P(("grp", "kv"), "tp", None, None))
    return jax.shard_map(
        per_device, mesh=mesh, in_specs=in_specs, out_specs=out_specs, check_vma=False
    )
```

time: 283 us -> 249 us (0.88)
  blocking collectives: 190 us -> 120 us
  starting transfers between devices: 42.9 us -> 62.6 us
  waiting for transfers between devices: 33.8 us -> 49.8 us
    all_gather x4 -> x1, blocking collectives: 126 us -> 23.5 us  [per_device(): lax.all_gather(hidden, 'kv', axis=0, tiled=True).reshape(cuts, rows, lanes)]
    all_to_all x2 -> x3, starting transfers between devices: 11.8 us -> 54.3 us  [from_everyone(): return lax.all_to_all(copies, axis, split_axis=0, concat_axis=0, tiled=True)]
    all_to_all x1 -> x3, blocking collectives: 31.3 us -> 65.3 us  [the longest x1 27.6 us: per_device(): down = lax.all_to_all(down.reshape(n_tp, -1, rows), 'tp', 0, 0, tiled=True)]
    all_to_all x2 -> x3, waiting for transfers between devices: 6.73 us -> 30 us  [from_everyone(): return lax.all_to_all(copies, axis, split_axis=0, concat_axis=0, tiled=True)]
    all_to_all x2 -> x1, starting transfers between devices: 20 us -> 6.96 us  [per_device(): got = lax.all_to_all(sent, 'kv', 0, 0, tiled=True)]
    unnamed x3 -> x1, starting transfers between devices: 11.1 us -> 1.31 us
    all_to_all x2 -> x1, waiting for transfers between devices: 25.9 us -> 19.8 us  [per_device(): got = lax.all_to_all(sent, 'kv', 0, 0, tiled=True)]
  transfers between devices with their start and end apart: 7 -> 5, of which waited for: 4 -> 4; matrix products, arithmetic and copies ran while one was open for 14% -> 1% of each run, Pallas kernels for 0% -> 0%
where the time goes in v1:
time: 249 us; the launch traced here: 248 us
  blocking collectives  120 us (48%)
  starting transfers between devices  62.6 us (25%)
  waiting for transfers between devices  49.8 us (20%)
  local copies, waits for them, and re-layouts  5.78 us (2%)
  matrix products  4.31 us (2%)
  other arithmetic  4.12 us (2%)
    all_to_all x3, starting transfers between devices, from_everyone(): return lax.all_to_all(copies, axis, split_axis=0, concat_axis=0, tiled=True)  54.3 us
    unnamed x1, blocking collectives  30.8 us
    all_to_all x3, waiting for transfers between devices, from_everyone(): return lax.all_to_all(copies, axis, split_axis=0, concat_axis=0, tiled=True)  30 us
    all_to_all x1, blocking collectives, per_device(): down = lax.all_to_all(down.reshape(n_tp, -1, rows), 'tp', 0, 0, tiled=True)  27.6 us
    all_gather x1, blocking collectives, per_device(): lax.all_gather(hidden, 'kv', axis=0, tiled=True).reshape(cuts, rows, lanes)  23.5 us
    all_to_all x1, blocking collectives, from_everyone(): return lax.all_to_all(copies, axis, split_axis=0, concat_axis=0, tiled=True)  21.8 us
    all_to_all x1, waiting for transfers between devices, per_device(): got = lax.all_to_all(sent, 'kv', 0, 0, tiled=True)  19.8 us
    all_to_all x1, blocking collectives, per_device(): lax.all_to_all(attn_part.reshape(n_tp, -1, rows), 'tp', 0, 0, tiled=True)  15.9 us
  transfers between devices with their start and end apart: 5, of which 4 were waited for; matrix products, arithmetic and copies ran while one was open for 1% of the time, Pallas kernels for 0%

profile of v1, /device:TPU:65, one launch (start us, length us, event | category | flops | bytes accessed | tf_op | source)
XLA Modules:
  0.0 248.0 jit_solution(14493385247816142615)
XLA Ops:
  0.7 1.5 broadcast_in_dim.8
  2.1 44.9 %all-to-all-start = ((bf16[16,16,320]{2,1,0:T(8,128)(2,1)}), bf16[16,16,320]{2,1,0:T(8,128)(2,1)S(1)}, u32[]{:S(2)}, u32[]{:S(2)}) async-start(bf16[16,16,320]{2,1,0:T(8,128)(2,1)} %broadcast_in_dim.8), calls=%async_computation | async-start | bytes 393216 | tf_op jit(solution)/shard_map/all_to_all | solution.py:16
  47.0 0.7 convert_element_type.173
  47.7 10.0 %all-to-all-done = bf16[16,16,320]{2,1,0:T(8,128)(2,1)S(1)} async-done(((bf16[16,16,320]{2,1,0:T(8,128)(2,1)}), bf16[16,16,320]{2,1,0:T(8,128)(2,1)S(1)}, u32[]{:S(2)}, u32[]{:S(2)}) %all-to-all-start) | async-done | bytes 163872 | tf_op jit(solution)/shard_map/all_to_all | solution.py:16
  59.1 0.8 pad_maximum_fusion
  60.0 7.0 %all-to-all-start.1 = ((bf16[16,24,512]{2,1,0:T(8,128)(2,1)}), bf16[16,24,512]{2,1,0:T(8,128)(2,1)S(1)}, u32[]{:S(2)}, u32[]{:S(2)}) async-start(bf16[16,24,512]{2,1,0:T(8,128)(2,1)} %pad_maximum_fusion), calls=%async_computation.1 | async-start | bytes 786432 | tf_op jit(solution)/shard_map/all_to_all | solution.py:99
  67.1 19.8 %all-to-all-done.1 = bf16[16,24,512]{2,1,0:T(8,128)(2,1)S(1)} async-done(((bf16[16,24,512]{2,1,0:T(8,128)(2,1)}), bf16[16,24,512]{2,1,0:T(8,128)(2,1)S(1)}, u32[]{:S(2)}, u32[]{:S(2)}) %all-to-all-start.1) | async-done | bytes 393248 | tf_op jit(solution)/shard_map/all_to_all | solution.py:99
  87.3 0.4 multiply_add_fusion
  87.8 1.2 fusion.1
  89.4 21.8 %all_to_all.35 = bf16[16,20,128]{2,1,0:T(8,128)(2,1)S(1)} all-to-all(bf16[16,20,128]{2,1,0:T(8,128)(2,1)S(1)} %broadcast_in_dim.9), channel_id=1, replica_groups=mesh['grp'=2,'kv'=16,'tp'=16] {'kv'}, dimensions={0} | all-to-all | bytes 163840 | tf_op jit(solution)/shard_map/all_to_all | solution.py:16
  111.6 15.9 %all_to_all.36 = bf16[16,16,320]{2,1,0:T(8,128)(2,1)S(1)} all-to-all(bf16[16,16,320]{2,1,0:T(8,128)(2,1)S(1)} %bitcast.129), channel_id=1, replica_groups=mesh['grp'=2,'kv'=16,'tp'=16] {'tp'}, dimensions={0} | all-to-all | bytes 327680 | tf_op jit(solution)/shard_map/all_to_all | solution.py:127
  127.5 0.7 broadcast_in_dim.10
  128.2 3.7 %all-to-all-start.4 = ((bf16[16,16,320]{2,1,0:T(8,128)(2,1)}), bf16[16,16,320]{2,1,0:T(8,128)(2,1)S(1)}, u32[]{:S(2)}, u32[]{:S(2)}) async-start(bf16[16,16,320]{2,1,0:T(8,128)(2,1)} %broadcast_in_dim.10), calls=%async_computation.4 | async-start | bytes 393216 | tf_op jit(solution)/shard_map/all_to_all | solution.py:16
  132.5 9.2 %all-to-all-done.4 = bf16[16,16,320]{2,1,0:T(8,128)(2,1)S(1)} async-done(((bf16[16,16,320]{2,1,0:T(8,128)(2,1)}), bf16[16,16,320]{2,1,0:T(8,128)(2,1)S(1)}, u32[]{:S(2)}, u32[]{:S(2)}) %all-to-all-start.4) | async-done | bytes 163872 | tf_op jit(solution)/shard_map/all_to_all | solution.py:16
  141.8 0.2 fusion.9
  142.1 0.3 fusion.8
  142.3 0.3 fusion.7
  142.6 0.3 fusion.6
  142.8 0.3 fusion.5
  143.1 0.3 fusion.4
  143.3 0.3 fusion.3
  143.6 30.8 %fusion = bf16[144,256]{1,0:T(8,128)(2,1)S(1)} fusion(bf16[2240,256]{1,0:T(8,128)(2,1)S(1)} %fusion.3), kind=kCustom, calls=%all-reduce-scatter | all-reduce-scatter fusion | flops 589825 | bytes 1222656
  174.4 1.3 collective-permute-start
  175.8 1.3 dynamic-slice.4
  177.7 0.6 broadcast_in_dim.11
  178.3 5.7 %all-to-all-start.5 = ((f32[16,1,320]{2,1,0:T(1,128)}), f32[16,1,320]{2,1,0:T(1,128)S(1)}, u32[]{:S(2)}, u32[]{:S(2)}) async-start(f32[16,1,320]{2,1,0:T(1,128)} %broadcast_in_dim.11), calls=%async_computation.5 | async-start | bytes 49152 | tf_op jit(solution)/shard_map/all_to_all | solution.py:16
  184.1 0.3 concatenate.40
  184.4 10.8 %all-to-all-done.5 = f32[16,1,320]{2,1,0:T(1,128)S(1)} async-done(((f32[16,1,320]{2,1,0:T(1,128)}), f32[16,1,320]{2,1,0:T(1,128)S(1)}, u32[]{:S(2)}, u32[]{:S(2)}) %all-to-all-start.5) | async-done | bytes 20512 | tf_op jit(solution)/shard_map/all_to_all | solution.py:16
  195.6 23.5 %all-gather = bf16[16,140,128]{2,1,0:T(8,128)(2,1)S(1)} all-gather(bf16[1,140,128]{2,1,0:T(8,128)(2,1)S(1)} %fusion.32), channel_id=1, replica_groups=mesh['grp'=2,'kv'=16,'tp'=16] {'kv'}, dimensions={0}, use_global_device_ids=true | all-gather | bytes 609280 | tf_op jit(solution)/shard_map/all_gather | solution.py:154
  219.2 0.3 fusion.10
  219.7 27.6 %all_to_all.37 = bf16[16,16,320]{2,1,0:T(8,128)(2,1)S(1)} all-to-all(bf16[16,16,320]{2,1,0:T(8,128)(2,1)S(1)} %bitcast.130), channel_id=1, replica_groups=mesh['grp'=2,'kv'=16,'tp'=16] {'tp'}, dimensions={0} | all-to-all | bytes 327680 | tf_op jit(solution)/shard_map/all_to_all | solution.py:161
  247.4 0.6 fusion.33
  (76 shorter events, 4.0 us)
Async XLA Ops:
  0.6 218.6 %copy-start = (bf16[896,256]{1,0:T(8,128)(2,1)S(1)}, bf16[896,256]{1,0:T(8,128)(2,1)}, u32[]{:S(2)}) copy-start(bf16[896,256]{1,0:T(8,128)(2,1)} %param.27) | copy-start | bytes 1376260
  0.6 57.5 %copy-start.7 = (bf16[256,128]{1,0:T(8,128)(2,1)S(1)}, bf16[256,128]{1,0:T(8,128)(2,1)}, u32[]{:S(2)}) copy-start(bf16[256,128]{1,0:T(8,128)(2,1)} %param.20) | copy-start | bytes 196612
  0.7 57.7 %copy-start.8 = (bf16[256,128]{1,0:T(8,128)(2,1)S(1)}, bf16[256,128]{1,0:T(8,128)(2,1)}, u32[]{:S(2)}) copy-start(bf16[256,128]{1,0:T(8,128)(2,1)} %param.19) | copy-start | bytes 196612
  2.1 56.5 %copy-start.9 = (bf16[256,128]{1,0:T(8,128)(2,1)S(1)}, bf16[256,128]{1,0:T(8,128)(2,1)}, u32[]{:S(2)}) copy-start(bf16[256,128]{1,0:T(8,128)(2,1)} %param.18) | copy-start | bytes 196612
  2.1 55.5 %all-to-all-start = ((bf16[16,16,320]{2,1,0:T(8,128)(2,1)}), bf16[16,16,320]{2,1,0:T(8,128)(2,1)S(1)}, u32[]{:S(2)}, u32[]{:S(2)}) async-start(bf16[16,16,320]{2,1,0:T(8,128)(2,1)} %broadcast_in_dim.8), calls=%async_computation | async-start | bytes 393216 | tf_op jit(solution)/shard_map/all_to_all | solution.py:16
  57.7 1.1 copy-start.10
  58.6 8.4 %copy-start.12 = (s32[20]{0:T(128)S(1)}, s32[20]{0:T(128)}, u32[]{:S(2)}) copy-start(s32[20]{0:T(128)} %param.15) | copy-start | bytes 244
  58.6 8.4 %copy-start.13 = (bf16[128]{0:T(256)(128)(2,1)S(1)}, bf16[128]{0:T(256)(128)(2,1)}, u32[]{:S(2)}) copy-start(bf16[128]{0:T(256)(128)(2,1)} %param.22) | copy-start | bytes 772
  59.1 28.2 %copy-start.2 = (f32[20,1,128,128]{3,2,1,0:T(8,128)S(1)}, f32[20,1,128,128]{3,2,1,0:T(8,128)}, u32[]{:S(2)}) copy-start(f32[20,1,128,128]{3,2,1,0:T(8,128)} %param.16) | copy-start | bytes 3932164
  60.0 26.9 %all-to-all-start.1 = ((bf16[16,24,512]{2,1,0:T(8,128)(2,1)}), bf16[16,24,512]{2,1,0:T(8,128)(2,1)S(1)}, u32[]{:S(2)}, u32[]{:S(2)}) async-start(bf16[16,24,512]{2,1,0:T(8,128)(2,1)} %pad_maximum_fusion), calls=%async_computation.1 | async-start | bytes 786432 | tf_op jit(solution)/shard_map/all_to_all | solution.py:99
  87.7 23.8 %copy-start.1 = (f32[20,1,128,128]{3,2,1,0:T(8,128)}, f32[20,1,128,128]{3,2,1,0:T(8,128)S(1)}, u32[]{:S(2)}) copy-start(f32[20,1,128,128]{3,2,1,0:T(8,128)S(1)} %multiply_add_fusion) | copy-start | bytes 3932164
  87.8 23.5 %copy-start.6 = (bf16[128,256]{1,0:T(8,128)(2,1)S(1)}, bf16[128,256]{1,0:T(8,128)(2,1)}, u32[]{:S(2)}) copy-start(bf16[128,256]{1,0:T(8,128)(2,1)} %param.23) | copy-start | bytes 196612
  89.0 38.5 %copy-start.5 = (bf16[320,16]{0,1:T(8,128)(2,1)S(1)}, bf16[320,16]{0,1:T(8,128)(2,1)}, u32[]{:S(2)}) copy-start(bf16[320,16]{0,1:T(8,128)(2,1)} %param.14) | copy-start | bytes 30724
  89.4 42.5 %copy-start.11 = (bf16[256]{0:T(256)(128)(2,1)S(1)}, bf16[256]{0:T(256)(128)(2,1)}, u32[]{:S(2)}) copy-start(bf16[256]{0:T(256)(128)(2,1)} %param.24) | copy-start | bytes 1540
  89.4 42.6 %copy-start.3 = (bf16[256,896]{1,0:T(8,128)(2,1)S(1)}, bf16[256,896]{1,0:T(8,128)(2,1)}, u32[]{:S(2)}) copy-start(bf16[256,896]{1,0:T(8,128)(2,1)} %param.25) | copy-start | bytes 1376260
  111.6 20.6 %copy-start.4 = (bf16[256,896]{1,0:T(8,128)(2,1)S(1)}, bf16[256,896]{1,0:T(8,128)(2,1)}, u32[]{:S(2)}) copy-start(bf16[256,896]{1,0:T(8,128)(2,1)} %param.26) | copy-start | bytes 1376260
  128.2 13.5 %all-to-all-start.4 = ((bf16[16,16,320]{2,1,0:T(8,128)(2,1)}), bf16[16,16,320]{2,1,0:T(8,128)(2,1)S(1)}, u32[]{:S(2)}, u32[]{:S(2)}) async-start(bf16[16,16,320]{2,1,0:T(8,128)(2,1)} %broadcast_in_dim.10), calls=%async_computation.4 | async-start | bytes 393216 | tf_op jit(solution)/shard_map/all_to_all | solution.py:16
  174.4 9.6 %collective-permute-start = (bf16[60,256]{1,0:T(8,128)(2,1)S(1)}, bf16[60,256]{1,0:T(8,128)(2,1)S(1)}, u32[]{:S(2)}, u32[]{:S(2)}) collective-permute-start(bf16[60,256]{1,0:T(8,128)(2,1)S(1)} %slice.105), channel_id=1, source_target_pairs={{0,16},{16,32},{32,48},{48,64},{64,80},{80,96},{96,112},{112,128},... | collective-permute-start | bytes 92168
  178.3 17.0 %all-to-all-start.5 = ((f32[16,1,320]{2,1,0:T(1,128)}), f32[16,1,320]{2,1,0:T(1,128)S(1)}, u32[]{:S(2)}, u32[]{:S(2)}) async-start(f32[16,1,320]{2,1,0:T(1,128)} %broadcast_in_dim.11), calls=%async_computation.5 | async-start | bytes 49152 | tf_op jit(solution)/shard_map/all_to_all | solution.py:16

commit v2 on v1

--- a/solution.py
+++ b/solution.py
@@ -1,6 +1,8 @@
 import jax
 import jax.numpy as jnp
 from jax import lax
+from jax.experimental import pallas as pl
+from jax.experimental.pallas import tpu as pltpu
 from jax.sharding import PartitionSpec as P
 
 
@@ -53,6 +55,54 @@
     normed = centred * lax.rsqrt(jnp.mean(centred * centred, axis=-1, keepdims=True) + epsilon)
     normed = normed.reshape(readout.shape[0], -1) * head_gain.astype(jnp.float32)
     return (new_memory, (normed * jax.nn.silu(gate_rows)).astype(jnp.bfloat16))
+
+
+def gate_and_up(order, wide, middle, parts):
+    blocks = len(wide)
+    units, block = wide[0].shape
+    rows = middle.shape[2]
+    share = units // (2 * parts)
+    tail = 8
+
+    def kernel(order_ref, *refs):
+        wide_refs, middle_ref, out_ref = refs[:blocks], refs[blocks], refs[blocks + 1]
+        total, squares = None, None
+        for m in range(blocks):
+            held = middle_ref[order_ref[m]]
+            value = held.astype(jnp.float32)
+            square = jnp.sum(value * value, axis=0, keepdims=True)
+            product = jnp.dot(wide_refs[m][...], held, preferred_element_type=jnp.float32)
+            total = product if total is None else total + product
+            squares = square if squares is None else squares + square
+        total = total.astype(jnp.bfloat16)
+        high, mid, low = in_three(squares)
+        ones = [high, mid, low, jnp.zeros_like(low)]
+        under = jnp.concatenate(
+            [
+                jnp.concatenate([ones[2 * r].astype(jnp.float32), ones[2 * r + 1].astype(jnp.float32)], axis=1)
+                for r in range(2)
+            ]
+            + [jnp.zeros((tail - 2, 2 * rows), jnp.float32)],
+            axis=0,
+        ).astype(jnp.bfloat16)
+        for a in range(parts):
+            for half in range(2):
+                start = (half * parts + a) * share
+                out_ref[a, :share, half * rows : (half + 1) * rows] = total[start : start + share]
+            out_ref[a, share:, :] = under
+
+    vmem = pl.BlockSpec(memory_space=pltpu.VMEM)
+    return pl.pallas_call(
+        kernel,
+        out_shape=jax.ShapeDtypeStruct((parts, share + tail, 2 * rows), jnp.bfloat16),
+        in_specs=[pl.BlockSpec(memory_space=pltpu.SMEM)] + [vmem] * (blocks + 1),
+        out_specs=vmem,
+        name="gate_and_up",
+        compiler_params=pltpu.CompilerParams(vmem_limit_bytes=16 * 2**20),
+        cost_estimate=pl.CostEstimate(
+            flops=2 * blocks * units * block * rows, bytes_accessed=2 * blocks * units * block, transcendentals=0
+        ),
+    )(order, *wide, middle)
 
 
 def per_device(
@@ -73,7 +123,6 @@
 ):
     f32, bf16 = jnp.float32, jnp.bfloat16
     n_kv, n_tp = lax.axis_size("kv"), lax.axis_size("tp")
-    kv = lax.axis_index("kv")
     rows = tokens.shape[0]
     own = memory.shape[0]
     heads_local = memory.shape[1]
@@ -83,12 +132,18 @@
     ff = w_up.shape[1]
 
     tok = tokens.T
-    gathered = from_everyone(tok, "tp").reshape(block, rows).astype(f32)
-    squares = jnp.sum(gathered * gathered, axis=0)
-    scaled = (gathered * norm_attn.astype(f32)[:, None]).astype(bf16)
+    gathered = lax.all_gather(tok, "tp", axis=0, tiled=True)
+    wide_tok = gathered.astype(f32)
+    squares = jnp.sum(wide_tok * wide_tok, axis=0)
+    gain = norm_attn.astype(f32)[:, None]
     parts = jnp.concatenate(
         [
-            lax.dot_general(scaled, w, (((0,), (0,)), ((), ())), preferred_element_type=f32)
+            lax.dot_general(
+                gathered,
+                (w.astype(f32) * gain).astype(bf16),
+                (((0,), (0,)), ((), ())),
+                preferred_element_type=f32,
+            )
             for w in (w_query, w_key, w_value, w_gate)
         ],
         axis=1,
@@ -120,6 +175,22 @@
         decay_rate,
     )
 
+    four = 4
+    fours = n_kv // four
+    near = [[a * four + i for i in range(four)] for a in range(fours)]
+    far = [[a * four + i for a in range(fours)] for i in range(four)]
+    share = ff // n_kv
+    place = lax.rem(lax.axis_index("kv"), four)
+    order = lax.bitwise_xor(place, jnp.arange(four))
+    gain = norm_mlp.astype(f32)[:, None]
+    wide = jnp.stack([(w.astype(f32) * gain).astype(bf16).T for w in (w_gate_mlp, w_up)])
+    wide = wide.reshape(2, fours, four, share, block).transpose(2, 0, 1, 3, 4)
+    wide = wide.reshape(four, 2 * fours * share, block)
+    wide = [lax.dynamic_index_in_dim(wide, order[j], 0, keepdims=False) for j in range(four)]
+    wide = [wide[0]] + [
+        lax.ppermute(wide[j], "kv", [(k, k ^ j) for k in range(n_kv)]) for j in range(1, four)
+    ]
+
     mixed_all = from_everyone(mixed, "kv").reshape(rows, width)
     attn_part = lax.dot_general(
         w_out, mixed_all, (((0,), (1,)), ((), ())), preferred_element_type=f32
@@ -127,36 +198,18 @@
     attn = lax.all_to_all(attn_part.reshape(n_tp, -1, rows), "tp", 0, 0, tiled=True)
     middle = (tok.astype(f32) + jnp.sum(attn.astype(f32), axis=0)).astype(bf16)
 
-    mid_all = from_everyone(middle, "tp").reshape(block, rows).astype(f32)
-    mid_squares = from_everyone(jnp.sum(mid_all * mid_all, axis=0)[None], "kv")
-    scaled_mid = (mid_all * norm_mlp.astype(f32)[:, None]).astype(bf16)
-    lanes = 128
-    cuts = ff // lanes
-    both = jnp.concatenate(
-        [w_gate_mlp.reshape(block, cuts, lanes), w_up.reshape(block, cuts, lanes)], axis=2
-    ).transpose(1, 0, 2)
-    terms = jnp.concatenate(
-        [
-            lax.dot_general(scaled_mid, both[c], (((0,), (0,)), ((), ())), preferred_element_type=f32)
-            for c in range(cuts)
-        ],
-        axis=0,
-    ).astype(bf16)
-    terms = lax.psum_scatter(terms, "kv", scatter_dimension=0, tiled=True)
-    terms = terms.astype(f32)
-    share = terms.shape[0]
-    totals = jnp.sum(mid_squares, axis=(0, 1))
-    inv_mlp = lax.rsqrt(totals / D + epsilon)
-    inv_mlp = lax.dynamic_slice_in_dim(
-        jnp.concatenate([inv_mlp, inv_mlp]), lax.rem(kv * share, rows), share, 0
-    )[:, None]
-    hidden = (jax.nn.silu(inv_mlp * terms[:, :lanes]) * (inv_mlp * terms[:, lanes:])).astype(bf16)
-    hidden = lax.all_gather(hidden, "kv", axis=0, tiled=True).reshape(cuts, rows, lanes)
+    copies = jnp.broadcast_to(middle, (four, *middle.shape))
+    mid_near = lax.all_to_all(copies, "kv", 0, 0, axis_index_groups=near, tiled=True)
+    mid_all = lax.all_gather(mid_near, "tp", axis=1, tiled=True)
+    both = gate_and_up(order, wide, mid_all, fours)
+    both = lax.all_to_all(both, "kv", 0, 0, axis_index_groups=far, tiled=True)
+    both = jnp.sum(both.astype(f32), axis=0)
+    totals = both[share, :rows] + both[share, rows:] + both[share + 1, :rows]
+    inv_mlp = lax.rsqrt(totals / D + epsilon)[None]
+    hidden = jax.nn.silu(inv_mlp * both[:share, :rows]) * (inv_mlp * both[:share, rows:])
+    hidden = lax.all_gather(hidden.astype(bf16), "kv", axis=0, tiled=True)
     down = lax.dot_general(
-        w_down,
-        hidden.transpose(1, 0, 2).reshape(rows, ff),
-        (((0,), (1,)), ((), ())),
-        preferred_element_type=f32,
+        w_down, hidden, (((0,), (0,)), ((), ())), preferred_element_type=f32
     ).astype(bf16)
     down = lax.all_to_all(down.reshape(n_tp, -1, rows), "tp", 0, 0, tiled=True)
     result = (middle.astype(f32) + jnp.sum(down.astype(f32), axis=0)).astype(bf16)

time: 249 us -> 241 us (0.968)
  blocking collectives: 120 us -> 149 us
  starting transfers between devices: 62.6 us -> 37.9 us
  waiting for transfers between devices: 49.8 us -> 31.4 us
  between operations: 1.8 us -> 8.85 us
    all_gather x1 -> x3, blocking collectives: 23.5 us -> 104 us  [the longest x1 56.3 us: per_device(): gathered = lax.all_gather(tok, 'tp', axis=0, tiled=True)]
    all_to_all x3 -> x1, starting transfers between devices: 54.3 us -> 11.1 us  [from_everyone(): return lax.all_to_all(copies, axis, split_axis=0, concat_axis=0, tiled=True)]
    unnamed x1 -> x0, blocking collectives: 30.8 us -> none
    all_to_all x3 -> x1, waiting for transfers between devices: 30 us -> 5.34 us  [from_everyone(): return lax.all_to_all(copies, axis, split_axis=0, concat_axis=0, tiled=True)]
    all_to_all x2 -> x1, blocking collectives: 37.6 us -> 22 us  [per_device(): both = lax.all_to_all(both, 'kv', 0, 0, axis_index_groups=far, tiled=True)]
    all_to_all x0 -> x2, starting transfers between devices: none -> 10.3 us  [the longest x1 6.97 us: per_device(): lax.all_to_all(attn_part.reshape(n_tp, -1, rows), 'tp', 0, 0, tiled=True)]
    ppermute x0 -> x3, starting transfers between devices: none -> 9.36 us  [per_device(): lax.ppermute(wide[j], 'kv', [(k, k ^ j) for k in range(n_kv)])]
    all_to_all x0 -> x2, waiting for transfers between devices: none -> 7.23 us  [the longest x1 7.23 us: per_device(): lax.all_to_all(attn_part.reshape(n_tp, -1, rows), 'tp', 0, 0, tiled=True)]
  transfers between devices with their start and end apart: 5 -> 7, of which waited for: 4 -> 3; matrix products, arithmetic and copies ran while one was open for 1% -> 1% of each run, Pallas kernels for 0% -> 0%
where the time goes in v2:
time: 241 us
  blocking collectives  149 us (62%)
  starting transfers between devices  37.9 us (16%)
  waiting for transfers between devices  31.4 us (13%)
  between operations  8.85 us (4%)
  matrix products  4.64 us (2%)
  other arithmetic  4.17 us (2%)
  local copies, waits for them, and re-layouts  3.78 us (2%)
    all_gather x1, blocking collectives, per_device(): gathered = lax.all_gather(tok, 'tp', axis=0, tiled=True)  56.3 us
    all_gather x1, blocking collectives, per_device(): hidden = lax.all_gather(hidden.astype(bf16), 'kv', axis=0, tiled=True)  30.5 us
    all_to_all x1, blocking collectives, per_device(): down = lax.all_to_all(down.reshape(n_tp, -1, rows), 'tp', 0, 0, tiled=True)  22.5 us
    all_to_all x1, blocking collectives, per_device(): both = lax.all_to_all(both, 'kv', 0, 0, axis_index_groups=far, tiled=True)  22 us
    all_to_all x1, waiting for transfers between devices, per_device(): got = lax.all_to_all(sent, 'kv', 0, 0, tiled=True)  18.8 us
    all_gather x1, blocking collectives, per_device(): mid_all = lax.all_gather(mid_near, 'tp', axis=1, tiled=True)  17.4 us
    all_to_all x1, starting transfers between devices, from_everyone(): return lax.all_to_all(copies, axis, split_axis=0, concat_axis=0, tiled=True)  11.1 us
    ppermute x3, starting transfers between devices, per_device(): lax.ppermute(wide[j], 'kv', [(k, k ^ j) for k in range(n_kv)])  9.36 us
  transfers between devices with their start and end apart: 7, of which 3 were waited for; matrix products, arithmetic and copies ran while one was open for 1% of the time, Pallas kernels for 0%

profile of v2, /device:TPU:65, one launch (start us, length us, event | category | flops | bytes accessed | tf_op | source)
XLA Modules:
  0.0 240.6 jit_solution(13644430005121410193)
XLA Ops:
  0.7 0.7 convert_element_type.177
  1.4 56.3 %all_gather.9 = bf16[256,320]{1,0:T(8,128)(2,1)S(1)} all-gather(bf16[16,320]{1,0:T(8,128)(2,1)} %bitcast.83), channel_id=1, replica_groups=mesh['grp'=2,'kv'=16,'tp'=16] {'tp'}, dimensions={0}, use_global_device_ids=true | all-gather | bytes 174080 | tf_op jit(solution)/shard_map/all_gather | solution.py:135
  57.9 1.1 fusion.7
  59.0 1.1 fusion.6
  60.2 0.3 fusion.5
  60.5 0.3 fusion.4
  61.0 0.8 pad_maximum_fusion
  61.8 7.1 %all-to-all-start = ((bf16[16,24,512]{2,1,0:T(8,128)(2,1)}), bf16[16,24,512]{2,1,0:T(8,128)(2,1)S(1)}, u32[]{:S(2)}, u32[]{:S(2)}) async-start(bf16[16,24,512]{2,1,0:T(8,128)(2,1)} %pad_maximum_fusion), calls=%async_computation | async-start | bytes 786432 | tf_op jit(solution)/shard_map/all_to_all | solution.py:154
  69.0 18.8 %all-to-all-done = bf16[16,24,512]{2,1,0:T(8,128)(2,1)S(1)} async-done(((bf16[16,24,512]{2,1,0:T(8,128)(2,1)}), bf16[16,24,512]{2,1,0:T(8,128)(2,1)S(1)}, u32[]{:S(2)}, u32[]{:S(2)}) %all-to-all-start) | async-done | bytes 393248 | tf_op jit(solution)/shard_map/all_to_all | solution.py:154
  88.3 0.4 multiply_add_fusion
  88.7 1.2 fusion
  90.3 0.7 broadcast_in_dim.4
  91.0 11.1 %all-to-all-start.1 = ((bf16[16,20,128]{2,1,0:T(8,128)(2,1)}), bf16[16,20,128]{2,1,0:T(8,128)(2,1)S(1)}, u32[]{:S(2)}, u32[]{:S(2)}) async-start(bf16[16,20,128]{2,1,0:T(8,128)(2,1)} %broadcast_in_dim.4), calls=%async_computation.1 | async-start | bytes 196608 | tf_op jit(solution)/shard_map/all_to_all | solution.py:18
  102.1 0.7 fusion.45
  107.9 0.2 copy.22
  108.2 0.2 copy.23
  108.4 5.3 %all-to-all-done.1 = bf16[16,20,128]{2,1,0:T(8,128)(2,1)S(1)} async-done(((bf16[16,20,128]{2,1,0:T(8,128)(2,1)}), bf16[16,20,128]{2,1,0:T(8,128)(2,1)S(1)}, u32[]{:S(2)}, u32[]{:S(2)}) %all-to-all-start.1) | async-done | bytes 81952 | tf_op jit(solution)/shard_map/all_to_all | solution.py:18
  114.0 0.8 copy.21
  114.8 7.0 %all-to-all-start.2 = ((bf16[16,16,320]{2,1,0:T(8,128)(2,1)}), bf16[16,16,320]{2,1,0:T(8,128)(2,1)S(1)}, u32[]{:S(2)}, u32[]{:S(2)}) async-start(bf16[16,16,320]{2,1,0:T(8,128)(2,1)} %bitcast.15), calls=%async_computation.2 | async-start | bytes 393216 | tf_op jit(solution)/shard_map/all_to_all | solution.py:198
  124.7 7.2 %all-to-all-done.2 = bf16[16,16,320]{2,1,0:T(8,128)(2,1)S(1)} async-done(((bf16[16,16,320]{2,1,0:T(8,128)(2,1)}), bf16[16,16,320]{2,1,0:T(8,128)(2,1)S(1)}, u32[]{:S(2)}, u32[]{:S(2)}) %all-to-all-start.2) | async-done | bytes 163872 | tf_op jit(solution)/shard_map/all_to_all | solution.py:198
  132.0 0.6 broadcast_in_dim.5
  132.6 3.4 %all-to-all-start.3 = ((bf16[4,16,320]{2,1,0:T(8,128)(2,1)}), bf16[4,16,320]{2,1,0:T(8,128)(2,1)S(1)}, u32[]{:S(2)}, u32[]{:S(2)}) async-start(bf16[4,16,320]{2,1,0:T(8,128)(2,1)} %broadcast_in_dim.5), calls=%async_computation.3 | async-start | bytes 98304 | tf_op jit(solution)/shard_map/all_to_all | solution.py:202
  136.1 5.1 %collective-permute-start.2 = (bf16[448,256]{1,0:T(8,128)(2,1)S(1)}, bf16[448,256]{1,0:T(8,128)(2,1)S(1)}, u32[]{:S(2)}, u32[]{:S(2)}) collective-permute-start(bf16[448,256]{1,0:T(8,128)(2,1)S(1)} %get-tuple-element.2), channel_id=1, source_target_pairs={{0,48},{16,32},{32,16},{48,0},{64,112},{80,96},{96,80},{112,64},{1... | collective-permute-start | bytes 688136 | tf_op jit(solution)/shard_map/ppermute | solution.py:191
  141.2 2.0 collective-permute-start.1
  143.2 2.3 collective-permute-start
  145.5 17.4 %all_gather.10.refs_4_ = bf16[4,256,320]{2,1,0:T(8,128)(2,1)S(1)} all-gather(bf16[4,16,320]{2,1,0:T(8,128)(2,1)S(1)} %all-to-all-done.3), channel_id=1, replica_groups=mesh['grp'=2,'kv'=16,'tp'=16] {'tp'}, dimensions={1}, use_global_device_ids=true | all-gather | bytes 696320 | tf_op jit(solution)/shard_map/all_gather | solution.py:203
  162.9 1.3 gate_and_up.1
  164.2 22.0 %all_to_all.30 = bf16[4,64,640]{2,1,0:T(8,128)(2,1)S(1)} all-to-all(bf16[4,64,640]{2,1,0:T(8,128)(2,1)S(1)} %gate_and_up.1), channel_id=1, replica_groups={{0,64,128,192},{16,80,144,208},{32,96,160,224},{48,112,176,240},{1,65,1..., dimensions={0} | all-to-all | bytes 655360 | tf_op jit(solution)/shard_map/all_to_all | solution.py:205
  186.5 30.5 %all_gather.11 = bf16[896,320]{1,0:T(8,128)(2,1)S(1)} all-gather(bf16[56,320]{1,0:T(8,128)(2,1)S(1)} %fusion.13), channel_id=1, replica_groups=mesh['grp'=2,'kv'=16,'tp'=16] {'kv'}, dimensions={0}, use_global_device_ids=true | all-gather | bytes 609280 | tf_op jit(solution)/shard_map/all_gather | solution.py:210
  217.0 0.4 fusion.2
  217.5 22.5 %all_to_all.31 = bf16[16,16,320]{2,1,0:T(8,128)(2,1)S(1)} all-to-all(bf16[16,16,320]{2,1,0:T(8,128)(2,1)S(1)} %bitcast.82), channel_id=1, replica_groups=mesh['grp'=2,'kv'=16,'tp'=16] {'tp'}, dimensions={0} | all-to-all | bytes 327680 | tf_op jit(solution)/shard_map/all_to_all | solution.py:214
  240.0 0.6 fusion.23
  (66 shorter events, 2.4 us)
Async XLA Ops:
  0.6 216.3 %copy-start = (bf16[896,256]{1,0:T(8,128)(2,1)S(1)}, bf16[896,256]{1,0:T(8,128)(2,1)}, u32[]{:S(2)}) copy-start(bf16[896,256]{1,0:T(8,128)(2,1)} %param.27) | copy-start | bytes 1376260
  0.6 59.6 %copy-start.7 = (bf16[256,128]{1,0:T(8,128)(2,1)S(1)}, bf16[256,128]{1,0:T(8,128)(2,1)}, u32[]{:S(2)}) copy-start(bf16[256,128]{1,0:T(8,128)(2,1)} %param.19) | copy-start | bytes 196612
  0.7 59.9 %copy-start.8 = (bf16[256,128]{1,0:T(8,128)(2,1)S(1)}, bf16[256,128]{1,0:T(8,128)(2,1)}, u32[]{:S(2)}) copy-start(bf16[256,128]{1,0:T(8,128)(2,1)} %param.18) | copy-start | bytes 196612
  60.5 8.5 %copy-start.9 = (s32[20]{0:T(128)S(1)}, s32[20]{0:T(128)}, u32[]{:S(2)}) copy-start(s32[20]{0:T(128)} %param.15) | copy-start | bytes 244
  60.5 8.5 %copy-start.10 = (bf16[128]{0:T(256)(128)(2,1)S(1)}, bf16[128]{0:T(256)(128)(2,1)}, u32[]{:S(2)}) copy-start(bf16[128]{0:T(256)(128)(2,1)} %param.22) | copy-start | bytes 772
  60.9 27.4 %copy-start.2 = (f32[20,1,128,128]{3,2,1,0:T(8,128)S(1)}, f32[20,1,128,128]{3,2,1,0:T(8,128)}, u32[]{:S(2)}) copy-start(f32[20,1,128,128]{3,2,1,0:T(8,128)} %param.16) | copy-start | bytes 3932164
  61.8 26.0 %all-to-all-start = ((bf16[16,24,512]{2,1,0:T(8,128)(2,1)}), bf16[16,24,512]{2,1,0:T(8,128)(2,1)S(1)}, u32[]{:S(2)}, u32[]{:S(2)}) async-start(bf16[16,24,512]{2,1,0:T(8,128)(2,1)} %pad_maximum_fusion), calls=%async_computation | async-start | bytes 786432 | tf_op jit(solution)/shard_map/all_to_all | solution.py:154
  88.7 19.5 %copy-start.1 = (f32[20,1,128,128]{3,2,1,0:T(8,128)}, f32[20,1,128,128]{3,2,1,0:T(8,128)S(1)}, u32[]{:S(2)}) copy-start(f32[20,1,128,128]{3,2,1,0:T(8,128)S(1)} %multiply_add_fusion) | copy-start | bytes 3932164
  88.7 19.2 %copy-start.11 = (bf16[256]{0:T(256)(128)(2,1)S(1)}, bf16[256]{0:T(256)(128)(2,1)}, u32[]{:S(2)}) copy-start(bf16[256]{0:T(256)(128)(2,1)} %param.24) | copy-start | bytes 1540
  88.7 19.2 %copy-start.3 = (bf16[256,896]{1,0:T(8,128)(2,1)S(1)}, bf16[256,896]{1,0:T(8,128)(2,1)}, u32[]{:S(2)}) copy-start(bf16[256,896]{1,0:T(8,128)(2,1)} %param.25) | copy-start | bytes 1376260
  88.7 19.5 %copy-start.4 = (bf16[256,896]{1,0:T(8,128)(2,1)S(1)}, bf16[256,896]{1,0:T(8,128)(2,1)}, u32[]{:S(2)}) copy-start(bf16[256,896]{1,0:T(8,128)(2,1)} %param.26) | copy-start | bytes 1376260
  89.9 23.8 %copy-start.6 = (bf16[128,256]{1,0:T(8,128)(2,1)S(1)}, bf16[128,256]{1,0:T(8,128)(2,1)}, u32[]{:S(2)}) copy-start(bf16[128,256]{1,0:T(8,128)(2,1)} %param.23) | copy-start | bytes 196612
  91.0 22.8 %all-to-all-start.1 = ((bf16[16,20,128]{2,1,0:T(8,128)(2,1)}), bf16[16,20,128]{2,1,0:T(8,128)(2,1)S(1)}, u32[]{:S(2)}, u32[]{:S(2)}) async-start(bf16[16,20,128]{2,1,0:T(8,128)(2,1)} %broadcast_in_dim.4), calls=%async_computation.1 | async-start | bytes 196608 | tf_op jit(solution)/shard_map/all_to_all | solution.py:18
  114.8 17.2 %all-to-all-start.2 = ((bf16[16,16,320]{2,1,0:T(8,128)(2,1)}), bf16[16,16,320]{2,1,0:T(8,128)(2,1)S(1)}, u32[]{:S(2)}, u32[]{:S(2)}) async-start(bf16[16,16,320]{2,1,0:T(8,128)(2,1)} %bitcast.15), calls=%async_computation.2 | async-start | bytes 393216 | tf_op jit(solution)/shard_map/all_to_all | solution.py:198
  122.0 9.9 %copy-start.5 = (bf16[320,16]{0,1:T(8,128)(2,1)S(1)}, bf16[320,16]{0,1:T(8,128)(2,1)}, u32[]{:S(2)}) copy-start(bf16[320,16]{0,1:T(8,128)(2,1)} %param.14) | copy-start | bytes 30724
  132.6 12.8 %all-to-all-start.3 = ((bf16[4,16,320]{2,1,0:T(8,128)(2,1)}), bf16[4,16,320]{2,1,0:T(8,128)(2,1)S(1)}, u32[]{:S(2)}, u32[]{:S(2)}) async-start(bf16[4,16,320]{2,1,0:T(8,128)(2,1)} %broadcast_in_dim.5), calls=%async_computation.3 | async-start | bytes 98304 | tf_op jit(solution)/shard_map/all_to_all | solution.py:202
  136.1 26.8 %collective-permute-start.2 = (bf16[448,256]{1,0:T(8,128)(2,1)S(1)}, bf16[448,256]{1,0:T(8,128)(2,1)S(1)}, u32[]{:S(2)}, u32[]{:S(2)}) collective-permute-start(bf16[448,256]{1,0:T(8,128)(2,1)S(1)} %get-tuple-element.2), channel_id=1, source_target_pairs={{0,48},{16,32},{32,16},{48,0},{64,112},{80,96},{96,80},{112,64},{1... | collective-permute-start | bytes 688136 | tf_op jit(solution)/shard_map/ppermute | solution.py:191
  141.2 21.7 %collective-permute-start.1 = (bf16[448,256]{1,0:T(8,128)(2,1)S(1)}, bf16[448,256]{1,0:T(8,128)(2,1)S(1)}, u32[]{:S(2)}, u32[]{:S(2)}) collective-permute-start(bf16[448,256]{1,0:T(8,128)(2,1)S(1)} %get-tuple-element.3), channel_id=1, source_target_pairs={{0,32},{16,48},{32,0},{48,16},{64,96},{80,112},{96,64},{112,80},{1... | collective-permute-start | bytes 688136 | tf_op jit(solution)/shard_map/ppermute | solution.py:191
  143.2 19.7 %collective-permute-start = (bf16[448,256]{1,0:T(8,128)(2,1)S(1)}, bf16[448,256]{1,0:T(8,128)(2,1)S(1)}, u32[]{:S(2)}, u32[]{:S(2)}) collective-permute-start(bf16[448,256]{1,0:T(8,128)(2,1)S(1)} %get-tuple-element.4), channel_id=1, source_target_pairs={{0,16},{16,0},{32,48},{48,32},{64,80},{80,64},{96,112},{112,96},{1... | collective-permute-start | bytes 688136 | tf_op jit(solution)/shard_map/ppermute | solution.py:191

commit v3 on v2

--- a/solution.py
+++ b/solution.py
@@ -180,15 +180,16 @@
     near = [[a * four + i for i in range(four)] for a in range(fours)]
     far = [[a * four + i for a in range(fours)] for i in range(four)]
     share = ff // n_kv
-    place = lax.rem(lax.axis_index("kv"), four)
-    order = lax.bitwise_xor(place, jnp.arange(four))
+    place = lax.div(lax.axis_index("kv"), four)
+    order = lax.bitwise_xor(place, jnp.arange(fours))
     gain = norm_mlp.astype(f32)[:, None]
     wide = jnp.stack([(w.astype(f32) * gain).astype(bf16).T for w in (w_gate_mlp, w_up)])
-    wide = wide.reshape(2, fours, four, share, block).transpose(2, 0, 1, 3, 4)
-    wide = wide.reshape(four, 2 * fours * share, block)
-    wide = [lax.dynamic_index_in_dim(wide, order[j], 0, keepdims=False) for j in range(four)]
+    wide = wide.reshape(2, fours, four * share, block).transpose(1, 0, 2, 3)
+    wide = wide.reshape(fours, 2 * four * share, block)
+    wide = [lax.dynamic_index_in_dim(wide, order[j], 0, keepdims=False) for j in range(fours)]
     wide = [wide[0]] + [
-        lax.ppermute(wide[j], "kv", [(k, k ^ j) for k in range(n_kv)]) for j in range(1, four)
+        lax.ppermute(wide[j], "kv", [(k, k ^ (j * four)) for k in range(n_kv)])
+        for j in range(1, fours)
     ]
 
     mixed_all = from_everyone(mixed, "kv").reshape(rows, width)
@@ -198,11 +199,11 @@
     attn = lax.all_to_all(attn_part.reshape(n_tp, -1, rows), "tp", 0, 0, tiled=True)
     middle = (tok.astype(f32) + jnp.sum(attn.astype(f32), axis=0)).astype(bf16)
 
-    copies = jnp.broadcast_to(middle, (four, *middle.shape))
-    mid_near = lax.all_to_all(copies, "kv", 0, 0, axis_index_groups=near, tiled=True)
-    mid_all = lax.all_gather(mid_near, "tp", axis=1, tiled=True)
-    both = gate_and_up(order, wide, mid_all, fours)
-    both = lax.all_to_all(both, "kv", 0, 0, axis_index_groups=far, tiled=True)
+    copies = jnp.broadcast_to(middle, (fours, *middle.shape))
+    mid_far = lax.all_to_all(copies, "kv", 0, 0, axis_index_groups=far, tiled=True)
+    mid_all = lax.all_gather(mid_far, "tp", axis=1, tiled=True)
+    both = gate_and_up(order, wide, mid_all, four)
+    both = lax.all_to_all(both, "kv", 0, 0, axis_index_groups=near, tiled=True)
     both = jnp.sum(both.astype(f32), axis=0)
     totals = both[share, :rows] + both[share, rows:] + both[share + 1, :rows]
     inv_mlp = lax.rsqrt(totals / D + epsilon)[None]

time: 241 us -> 255 us (1.058)
  waiting for transfers between devices: 31.4 us -> 48.7 us
  blocking collectives: 149 us -> 137 us
  starting transfers between devices: 37.9 us -> 45.6 us
    ppermute x3, waiting for transfers between devices: 0.01 us -> 17.3 us  [per_device(): lax.ppermute(wide[j], 'kv', [(k, k ^ j * four) for k in range(n_kv)])]
    ppermute x3, starting transfers between devices: 9.36 us -> 16.3 us  [per_device(): lax.ppermute(wide[j], 'kv', [(k, k ^ j * four) for k in range(n_kv)])]
    all_gather x1, blocking collectives: 30.5 us -> 23.7 us  [per_device(): hidden = lax.all_gather(hidden.astype(bf16), 'kv', axis=0, tiled=True)]
    all_to_all x1, blocking collectives: 22 us -> 17.9 us  [per_device(): both = lax.all_to_all(both, 'kv', 0, 0, axis_index_groups=near, tiled=True)]
  transfers between devices with their start and end apart: 7 -> 7, of which waited for: 3 -> 5; matrix products, arithmetic and copies ran while one was open for 1% -> 1% of each run, Pallas kernels for 0% -> 0%
where the time goes in v3:
time: 255 us; the launch traced here: 254 us
  blocking collectives  137 us (54%)
  waiting for transfers between devices  48.7 us (19%)
  starting transfers between devices  45.6 us (18%)
  between operations  8.82 us (3%)
  matrix products  4.64 us (2%)
  other arithmetic  4.17 us (2%)
  local copies, waits for them, and re-layouts  3.75 us (1%)
    all_gather x1, blocking collectives, per_device(): gathered = lax.all_gather(tok, 'tp', axis=0, tiled=True)  56.3 us
    all_gather x1, blocking collectives, per_device(): hidden = lax.all_gather(hidden.astype(bf16), 'kv', axis=0, tiled=True)  23.7 us
    all_to_all x1, blocking collectives, per_device(): down = lax.all_to_all(down.reshape(n_tp, -1, rows), 'tp', 0, 0, tiled=True)  21.5 us
    all_to_all x1, waiting for transfers between devices, per_device(): got = lax.all_to_all(sent, 'kv', 0, 0, tiled=True)  18.8 us
    all_to_all x1, blocking collectives, per_device(): both = lax.all_to_all(both, 'kv', 0, 0, axis_index_groups=near, tiled=True)  17.9 us
    all_gather x1, blocking collectives, per_device(): mid_all = lax.all_gather(mid_far, 'tp', axis=1, tiled=True)  17.7 us
    ppermute x3, waiting for transfers between devices, per_device(): lax.ppermute(wide[j], 'kv', [(k, k ^ j * four) for k in range(n_kv)])  17.3 us
    ppermute x3, starting transfers between devices, per_device(): lax.ppermute(wide[j], 'kv', [(k, k ^ j * four) for k in range(n_kv)])  16.3 us
  transfers between devices with their start and end apart: 7, of which 5 were waited for; matrix products, arithmetic and copies ran while one was open for 1% of the time, Pallas kernels for 0%

profile of v3, /device:TPU:65, one launch (start us, length us, event | category | flops | bytes accessed | tf_op | source)
XLA Modules:
  0.0 253.9 jit_solution(13466620704988702883)
XLA Ops:
  0.7 0.7 convert_element_type.177
  1.4 56.3 %all_gather.9 = bf16[256,320]{1,0:T(8,128)(2,1)S(1)} all-gather(bf16[16,320]{1,0:T(8,128)(2,1)} %bitcast.83), channel_id=1, replica_groups=mesh['grp'=2,'kv'=16,'tp'=16] {'tp'}, dimensions={0}, use_global_device_ids=true | all-gather | bytes 174080 | tf_op jit(solution)/shard_map/all_gather | solution.py:135
  57.9 1.1 fusion.7
  59.0 1.1 fusion.6
  60.2 0.3 fusion.5
  60.5 0.3 fusion.4
  61.0 0.8 pad_maximum_fusion
  61.8 7.1 %all-to-all-start = ((bf16[16,24,512]{2,1,0:T(8,128)(2,1)}), bf16[16,24,512]{2,1,0:T(8,128)(2,1)S(1)}, u32[]{:S(2)}, u32[]{:S(2)}) async-start(bf16[16,24,512]{2,1,0:T(8,128)(2,1)} %pad_maximum_fusion), calls=%async_computation | async-start | bytes 786432 | tf_op jit(solution)/shard_map/all_to_all | solution.py:154
  69.0 18.8 %all-to-all-done = bf16[16,24,512]{2,1,0:T(8,128)(2,1)S(1)} async-done(((bf16[16,24,512]{2,1,0:T(8,128)(2,1)}), bf16[16,24,512]{2,1,0:T(8,128)(2,1)S(1)}, u32[]{:S(2)}, u32[]{:S(2)}) %all-to-all-start) | async-done | bytes 393248 | tf_op jit(solution)/shard_map/all_to_all | solution.py:154
  88.3 0.4 multiply_add_fusion
  88.7 1.2 fusion
  90.3 0.7 broadcast_in_dim.4
  91.0 11.1 %all-to-all-start.1 = ((bf16[16,20,128]{2,1,0:T(8,128)(2,1)}), bf16[16,20,128]{2,1,0:T(8,128)(2,1)S(1)}, u32[]{:S(2)}, u32[]{:S(2)}) async-start(bf16[16,20,128]{2,1,0:T(8,128)(2,1)} %broadcast_in_dim.4), calls=%async_computation.1 | async-start | bytes 196608 | tf_op jit(solution)/shard_map/all_to_all | solution.py:18
  102.1 0.7 fusion.45
  108.4 5.3 %all-to-all-done.1 = bf16[16,20,128]{2,1,0:T(8,128)(2,1)S(1)} async-done(((bf16[16,20,128]{2,1,0:T(8,128)(2,1)}), bf16[16,20,128]{2,1,0:T(8,128)(2,1)S(1)}, u32[]{:S(2)}, u32[]{:S(2)}) %all-to-all-start.1) | async-done | bytes 81952 | tf_op jit(solution)/shard_map/all_to_all | solution.py:18
  114.0 0.8 copy.21
  114.8 7.0 %all-to-all-start.2 = ((bf16[16,16,320]{2,1,0:T(8,128)(2,1)}), bf16[16,16,320]{2,1,0:T(8,128)(2,1)S(1)}, u32[]{:S(2)}, u32[]{:S(2)}) async-start(bf16[16,16,320]{2,1,0:T(8,128)(2,1)} %bitcast.15), calls=%async_computation.2 | async-start | bytes 393216 | tf_op jit(solution)/shard_map/all_to_all | solution.py:199
  124.7 7.2 %all-to-all-done.2 = bf16[16,16,320]{2,1,0:T(8,128)(2,1)S(1)} async-done(((bf16[16,16,320]{2,1,0:T(8,128)(2,1)}), bf16[16,16,320]{2,1,0:T(8,128)(2,1)S(1)}, u32[]{:S(2)}, u32[]{:S(2)}) %all-to-all-start.2) | async-done | bytes 163872 | tf_op jit(solution)/shard_map/all_to_all | solution.py:199
  132.0 0.6 broadcast_in_dim.5
  132.6 4.2 %all-to-all-start.3 = ((bf16[4,16,320]{2,1,0:T(8,128)(2,1)}), bf16[4,16,320]{2,1,0:T(8,128)(2,1)S(1)}, u32[]{:S(2)}, u32[]{:S(2)}) async-start(bf16[4,16,320]{2,1,0:T(8,128)(2,1)} %broadcast_in_dim.5), calls=%async_computation.3 | async-start | bytes 98304 | tf_op jit(solution)/shard_map/all_to_all | solution.py:203
  136.9 7.3 %collective-permute-start.2 = (bf16[448,256]{1,0:T(8,128)(2,1)S(1)}, bf16[448,256]{1,0:T(8,128)(2,1)S(1)}, u32[]{:S(2)}, u32[]{:S(2)}) collective-permute-start(bf16[448,256]{1,0:T(8,128)(2,1)S(1)} %get-tuple-element.2), channel_id=1, source_target_pairs={{0,192},{16,208},{32,224},{48,240},{64,128},{80,144},{96,160},{112... | collective-permute-start | bytes 688136 | tf_op jit(solution)/shard_map/ppermute | solution.py:191
  144.2 7.0 %collective-permute-start.1 = (bf16[448,256]{1,0:T(8,128)(2,1)S(1)}, bf16[448,256]{1,0:T(8,128)(2,1)S(1)}, u32[]{:S(2)}, u32[]{:S(2)}) collective-permute-start(bf16[448,256]{1,0:T(8,128)(2,1)S(1)} %get-tuple-element.3), channel_id=1, source_target_pairs={{0,128},{16,144},{32,160},{48,176},{64,192},{80,208},{96,224},{112... | collective-permute-start | bytes 688136 | tf_op jit(solution)/shard_map/ppermute | solution.py:191
  151.2 2.0 collective-permute-start
  153.2 17.7 %all_gather.10.refs_4_ = bf16[4,256,320]{2,1,0:T(8,128)(2,1)S(1)} all-gather(bf16[4,16,320]{2,1,0:T(8,128)(2,1)S(1)} %all-to-all-done.3), channel_id=1, replica_groups=mesh['grp'=2,'kv'=16,'tp'=16] {'tp'}, dimensions={1}, use_global_device_ids=true | all-gather | bytes 696320 | tf_op jit(solution)/shard_map/all_gather | solution.py:204
  170.9 13.1 %collective-permute-done.2.refs_3_ = bf16[448,256]{1,0:T(8,128)(2,1)S(1)} collective-permute-done((bf16[448,256]{1,0:T(8,128)(2,1)S(1)}, bf16[448,256]{1,0:T(8,128)(2,1)S(1)}, u32[]{:S(2)}, u32[]{:S(2)}) %collective-permute-start.2) | collective-permute-done | bytes 229408 | tf_op jit(solution)/shard_map/ppermute | solution.py:191
  184.0 4.2 %collective-permute-done.refs_1_ = bf16[448,256]{1,0:T(8,128)(2,1)S(1)} collective-permute-done((bf16[448,256]{1,0:T(8,128)(2,1)S(1)}, bf16[448,256]{1,0:T(8,128)(2,1)S(1)}, u32[]{:S(2)}, u32[]{:S(2)}) %collective-permute-start) | collective-permute-done | bytes 229408 | tf_op jit(solution)/shard_map/ppermute | solution.py:191
  188.1 1.3 gate_and_up.1
  189.4 17.9 %all_to_all.30 = bf16[4,64,640]{2,1,0:T(8,128)(2,1)S(1)} all-to-all(bf16[4,64,640]{2,1,0:T(8,128)(2,1)S(1)} %gate_and_up.1), channel_id=1, replica_groups={{0,16,32,48},{64,80,96,112},{128,144,160,176},{192,208,224,240},{1,17,3..., dimensions={0} | all-to-all | bytes 655360 | tf_op jit(solution)/shard_map/all_to_all | solution.py:206
  207.5 23.7 %all_gather.11 = bf16[896,320]{1,0:T(8,128)(2,1)S(1)} all-gather(bf16[56,320]{1,0:T(8,128)(2,1)S(1)} %fusion.13), channel_id=1, replica_groups=mesh['grp'=2,'kv'=16,'tp'=16] {'kv'}, dimensions={0}, use_global_device_ids=true | all-gather | bytes 609280 | tf_op jit(solution)/shard_map/all_gather | solution.py:211
  231.2 0.4 fusion.2
  231.8 21.5 %all_to_all.31 = bf16[16,16,320]{2,1,0:T(8,128)(2,1)S(1)} all-to-all(bf16[16,16,320]{2,1,0:T(8,128)(2,1)S(1)} %bitcast.82), channel_id=1, replica_groups=mesh['grp'=2,'kv'=16,'tp'=16] {'tp'}, dimensions={0} | all-to-all | bytes 327680 | tf_op jit(solution)/shard_map/all_to_all | solution.py:215
  253.3 0.6 fusion.23
  (66 shorter events, 2.8 us)
Async XLA Ops:
  0.6 230.6 %copy-start = (bf16[896,256]{1,0:T(8,128)(2,1)S(1)}, bf16[896,256]{1,0:T(8,128)(2,1)}, u32[]{:S(2)}) copy-start(bf16[896,256]{1,0:T(8,128)(2,1)} %param.27) | copy-start | bytes 1376260
  0.6 59.6 %copy-start.7 = (bf16[256,128]{1,0:T(8,128)(2,1)S(1)}, bf16[256,128]{1,0:T(8,128)(2,1)}, u32[]{:S(2)}) copy-start(bf16[256,128]{1,0:T(8,128)(2,1)} %param.19) | copy-start | bytes 196612
  0.7 59.9 %copy-start.8 = (bf16[256,128]{1,0:T(8,128)(2,1)S(1)}, bf16[256,128]{1,0:T(8,128)(2,1)}, u32[]{:S(2)}) copy-start(bf16[256,128]{1,0:T(8,128)(2,1)} %param.18) | copy-start | bytes 196612
  60.5 8.5 %copy-start.9 = (s32[20]{0:T(128)S(1)}, s32[20]{0:T(128)}, u32[]{:S(2)}) copy-start(s32[20]{0:T(128)} %param.15) | copy-start | bytes 244
  60.5 8.5 %copy-start.10 = (bf16[128]{0:T(256)(128)(2,1)S(1)}, bf16[128]{0:T(256)(128)(2,1)}, u32[]{:S(2)}) copy-start(bf16[128]{0:T(256)(128)(2,1)} %param.22) | copy-start | bytes 772
  60.9 27.4 %copy-start.2 = (f32[20,1,128,128]{3,2,1,0:T(8,128)S(1)}, f32[20,1,128,128]{3,2,1,0:T(8,128)}, u32[]{:S(2)}) copy-start(f32[20,1,128,128]{3,2,1,0:T(8,128)} %param.16) | copy-start | bytes 3932164
  61.8 26.0 %all-to-all-start = ((bf16[16,24,512]{2,1,0:T(8,128)(2,1)}), bf16[16,24,512]{2,1,0:T(8,128)(2,1)S(1)}, u32[]{:S(2)}, u32[]{:S(2)}) async-start(bf16[16,24,512]{2,1,0:T(8,128)(2,1)} %pad_maximum_fusion), calls=%async_computation | async-start | bytes 786432 | tf_op jit(solution)/shard_map/all_to_all | solution.py:154
  88.7 19.5 %copy-start.1 = (f32[20,1,128,128]{3,2,1,0:T(8,128)}, f32[20,1,128,128]{3,2,1,0:T(8,128)S(1)}, u32[]{:S(2)}) copy-start(f32[20,1,128,128]{3,2,1,0:T(8,128)S(1)} %multiply_add_fusion) | copy-start | bytes 3932164
  88.7 19.2 %copy-start.11 = (bf16[256]{0:T(256)(128)(2,1)S(1)}, bf16[256]{0:T(256)(128)(2,1)}, u32[]{:S(2)}) copy-start(bf16[256]{0:T(256)(128)(2,1)} %param.24) | copy-start | bytes 1540
  88.7 19.2 %copy-start.3 = (bf16[256,896]{1,0:T(8,128)(2,1)S(1)}, bf16[256,896]{1,0:T(8,128)(2,1)}, u32[]{:S(2)}) copy-start(bf16[256,896]{1,0:T(8,128)(2,1)} %param.25) | copy-start | bytes 1376260
  88.7 19.5 %copy-start.4 = (bf16[256,896]{1,0:T(8,128)(2,1)S(1)}, bf16[256,896]{1,0:T(8,128)(2,1)}, u32[]{:S(2)}) copy-start(bf16[256,896]{1,0:T(8,128)(2,1)} %param.26) | copy-start | bytes 1376260
  89.9 23.8 %copy-start.6 = (bf16[128,256]{1,0:T(8,128)(2,1)S(1)}, bf16[128,256]{1,0:T(8,128)(2,1)}, u32[]{:S(2)}) copy-start(bf16[128,256]{1,0:T(8,128)(2,1)} %param.23) | copy-start | bytes 196612
  91.0 22.8 %all-to-all-start.1 = ((bf16[16,20,128]{2,1,0:T(8,128)(2,1)}), bf16[16,20,128]{2,1,0:T(8,128)(2,1)S(1)}, u32[]{:S(2)}, u32[]{:S(2)}) async-start(bf16[16,20,128]{2,1,0:T(8,128)(2,1)} %broadcast_in_dim.4), calls=%async_computation.1 | async-start | bytes 196608 | tf_op jit(solution)/shard_map/all_to_all | solution.py:18
  114.8 17.2 %all-to-all-start.2 = ((bf16[16,16,320]{2,1,0:T(8,128)(2,1)}), bf16[16,16,320]{2,1,0:T(8,128)(2,1)S(1)}, u32[]{:S(2)}, u32[]{:S(2)}) async-start(bf16[16,16,320]{2,1,0:T(8,128)(2,1)} %bitcast.15), calls=%async_computation.2 | async-start | bytes 393216 | tf_op jit(solution)/shard_map/all_to_all | solution.py:199
  122.0 9.9 %copy-start.5 = (bf16[320,16]{0,1:T(8,128)(2,1)S(1)}, bf16[320,16]{0,1:T(8,128)(2,1)}, u32[]{:S(2)}) copy-start(bf16[320,16]{0,1:T(8,128)(2,1)} %param.14) | copy-start | bytes 30724
  132.6 20.5 %all-to-all-start.3 = ((bf16[4,16,320]{2,1,0:T(8,128)(2,1)}), bf16[4,16,320]{2,1,0:T(8,128)(2,1)S(1)}, u32[]{:S(2)}, u32[]{:S(2)}) async-start(bf16[4,16,320]{2,1,0:T(8,128)(2,1)} %broadcast_in_dim.5), calls=%async_computation.3 | async-start | bytes 98304 | tf_op jit(solution)/shard_map/all_to_all | solution.py:203
  136.9 47.1 %collective-permute-start.2 = (bf16[448,256]{1,0:T(8,128)(2,1)S(1)}, bf16[448,256]{1,0:T(8,128)(2,1)S(1)}, u32[]{:S(2)}, u32[]{:S(2)}) collective-permute-start(bf16[448,256]{1,0:T(8,128)(2,1)S(1)} %get-tuple-element.2), channel_id=1, source_target_pairs={{0,192},{16,208},{32,224},{48,240},{64,128},{80,144},{96,160},{112... | collective-permute-start | bytes 688136 | tf_op jit(solution)/shard_map/ppermute | solution.py:191
  144.2 39.8 %collective-permute-start.1 = (bf16[448,256]{1,0:T(8,128)(2,1)S(1)}, bf16[448,256]{1,0:T(8,128)(2,1)S(1)}, u32[]{:S(2)}, u32[]{:S(2)}) collective-permute-start(bf16[448,256]{1,0:T(8,128)(2,1)S(1)} %get-tuple-element.3), channel_id=1, source_target_pairs={{0,128},{16,144},{32,160},{48,176},{64,192},{80,208},{96,224},{112... | collective-permute-start | bytes 688136 | tf_op jit(solution)/shard_map/ppermute | solution.py:191
  151.2 36.9 %collective-permute-start = (bf16[448,256]{1,0:T(8,128)(2,1)S(1)}, bf16[448,256]{1,0:T(8,128)(2,1)S(1)}, u32[]{:S(2)}, u32[]{:S(2)}) collective-permute-start(bf16[448,256]{1,0:T(8,128)(2,1)S(1)} %get-tuple-element.4), channel_id=1, source_target_pairs={{0,64},{16,80},{32,96},{48,112},{64,0},{80,16},{96,32},{112,48},{1... | collective-permute-start | bytes 688136 | tf_op jit(solution)/shard_map/ppermute | solution.py:191

commit v4 on v2

--- a/solution.py
+++ b/solution.py
@@ -13,11 +13,6 @@
 epsilon = 1e-06
 
 
-def from_everyone(array, axis):
-    copies = jnp.broadcast_to(array, (lax.axis_size(axis), *array.shape))
-    return lax.all_to_all(copies, axis, split_axis=0, concat_axis=0, tiled=True)
-
-
 def in_three(values):
     high = values.astype(jnp.bfloat16)
     rest = values - high.astype(jnp.float32)
@@ -26,35 +21,115 @@
     return high, mid, low
 
 
-def rotate(values, cosine, sine):
-    half_width = values.shape[-1] // 2
-    first = values[..., :half_width]
-    second = values[..., half_width:]
-    return jnp.concatenate(
-        [first * cosine - second * sine, second * cosine + first * sine], axis=-1
-    )
-
-
 def head_decay(head_index):
     exponent = -5.0 - head_index.astype(jnp.float32) * (7.0 / max(HEADS - 1, 1))
     return 1.0 - jnp.exp2(exponent)
 
 
-def retain(memory, queries, key_rows, value_rows, gate_rows, head_gain, decay_rate):
-    new_memory = (
-        decay_rate[None, :, None, None] * memory
-        + key_rows[:, :, :, None] * value_rows[:, :, None, :]
-    )
-    readout = jnp.einsum(
-        "bhd,bhde->bhe",
-        queries * queries.shape[-1] ** (-0.5),
-        new_memory,
-        precision=lax.Precision.HIGHEST,
-    )
-    centred = readout - jnp.mean(readout, axis=-1, keepdims=True)
-    normed = centred * lax.rsqrt(jnp.mean(centred * centred, axis=-1, keepdims=True) + epsilon)
-    normed = normed.reshape(readout.shape[0], -1) * head_gain.astype(jnp.float32)
-    return (new_memory, (normed * jax.nn.silu(gate_rows)).astype(jnp.bfloat16))
+VMEM = pl.BlockSpec(memory_space=pltpu.VMEM)
+SMEM = pl.BlockSpec(memory_space=pltpu.SMEM)
+LIMIT = pltpu.CompilerParams(vmem_limit_bytes=16 * 2**20)
+
+
+def project(gathered, norm, weights, pieces):
+    block, rows = gathered.shape
+    width = weights[0].shape[1]
+    count = len(weights)
+    own = rows // pieces
+    height = -(-(own + 3) // 8) * 8
+
+    def kernel(tokens_ref, norm_ref, *refs):
+        out_ref, held_ref, arrived = refs[count:]
+        copies = [
+            pltpu.make_async_copy(refs[c], held_ref.at[c], arrived.at[c]) for c in range(count)
+        ]
+        for copy in copies:
+            copy.start()
+        value = tokens_ref[...].astype(jnp.float32)
+        squares = jnp.sum(value * value, axis=0, keepdims=True)
+        gain = jnp.broadcast_to(norm_ref[...].astype(jnp.float32), (128, block)).T[:, :1]
+        scaled = (value * gain).astype(jnp.bfloat16)
+        under = [term.astype(jnp.float32) for term in in_three(squares)]
+        under = jnp.concatenate(under + [jnp.zeros((height - own - 3, rows), jnp.float32)], axis=0)
+        under = jnp.concatenate(
+            [under, jnp.zeros((height - own, count * width - rows), jnp.float32)], axis=1
+        )
+        for c in range(count):
+            copies[c].wait()
+            product = lax.dot_general(
+                scaled, held_ref[c], (((0,), (0,)), ((), ())), preferred_element_type=jnp.float32
+            )
+            span = slice(c * width, (c + 1) * width)
+            for p in range(pieces):
+                piece = jnp.concatenate([product[p * own : (p + 1) * own], under[:, span]], axis=0)
+                out_ref[p, :, span] = piece.astype(jnp.bfloat16)
+
+    return pl.pallas_call(
+        kernel,
+        out_shape=jax.ShapeDtypeStruct((pieces, height, count * width), jnp.bfloat16),
+        in_specs=[VMEM] * 2 + [pl.BlockSpec(memory_space=pl.ANY)] * count,
+        out_specs=VMEM,
+        scratch_shapes=[
+            pltpu.VMEM((count, block, width), jnp.bfloat16),
+            pltpu.SemaphoreType.DMA((count,)),
+        ],
+        name="project",
+        compiler_params=LIMIT,
+        cost_estimate=pl.CostEstimate(
+            flops=2 * count * block * width * rows, bytes_accessed=2 * gathered.size, transcendentals=0
+        ),
+    )(gathered, norm, *weights)
+
+
+def attend(scalars, start, parts, cosine, sine, memory, head_gain, rows):
+    pieces, _, _ = parts.shape
+    own, size, _ = memory.shape
+
+    def kernel(scalars_ref, start_ref, parts_ref, cos_ref, sin_ref, memory_ref, gain_ref, *refs):
+        mixed_ref, keys_ref, values_ref, read_ref = refs
+        summed = parts_ref[0].astype(jnp.float32)
+        for p in range(1, pieces):
+            summed = summed + parts_ref[p].astype(jnp.float32)
+        total = summed[own : own + 1, :rows] + summed[own + 1 : own + 2, :rows]
+        total = total + summed[own + 2 : own + 3, :rows]
+        lane = lax.broadcasted_iota(jnp.int32, (own, rows), 1)
+        line = lax.broadcasted_iota(jnp.int32, (own, rows), 0) + start_ref[0]
+        total = jnp.sum(jnp.where(lane == line, total, 0.0), axis=1, keepdims=True)
+        scale = lax.rsqrt(total / D + epsilon)
+        query, key, value, gate = (
+            summed[:own, i * size : (i + 1) * size] * scale for i in range(4)
+        )
+        query, key = (
+            x * cos_ref[...] + pltpu.roll(x, size // 2, 1) * sin_ref[...] for x in (query, key)
+        )
+        query = query * size ** (-0.5)
+        columns = jnp.concatenate([query, jnp.zeros((size - own, size), jnp.float32)], axis=0).T
+        for b in range(own):
+            read_ref[b : b + 1] = jnp.sum(columns[:, b : b + 1] * memory_ref[b], axis=0, keepdims=True)
+        decay = scalars_ref[0]
+        readout = decay * read_ref[...] + jnp.sum(query * key, axis=1, keepdims=True) * value
+        centred = readout - jnp.mean(readout, axis=1, keepdims=True)
+        normed = centred * lax.rsqrt(jnp.mean(centred * centred, axis=1, keepdims=True) + epsilon)
+        normed = normed * gain_ref[...].astype(jnp.float32)
+        mixed = (normed * (gate / (1.0 + jnp.exp(-gate)))).astype(jnp.bfloat16)
+        for p in range(pieces):
+            mixed_ref[p] = mixed
+        keys_ref[...] = key
+        values_ref[...] = value
+
+    rows_type = jax.ShapeDtypeStruct((own, size), jnp.float32)
+    return pl.pallas_call(
+        kernel,
+        out_shape=(jax.ShapeDtypeStruct((pieces, own, size), jnp.bfloat16), rows_type, rows_type),
+        in_specs=[SMEM, SMEM] + [VMEM] * 5,
+        out_specs=(VMEM,) * 3,
+        scratch_shapes=[pltpu.VMEM((own, size), jnp.float32)],
+        name="attend",
+        compiler_params=LIMIT,
+        cost_estimate=pl.CostEstimate(
+            flops=2 * memory.size, bytes_accessed=4 * memory.size, transcendentals=2 * own * size
+        ),
+    )(scalars, start, parts, cosine, sine, memory, head_gain)
 
 
 def gate_and_up(order, wide, middle, parts):
@@ -91,14 +166,13 @@
                 out_ref[a, :share, half * rows : (half + 1) * rows] = total[start : start + share]
             out_ref[a, share:, :] = under
 
-    vmem = pl.BlockSpec(memory_space=pltpu.VMEM)
     return pl.pallas_call(
         kernel,
         out_shape=jax.ShapeDtypeStruct((parts, share + tail, 2 * rows), jnp.bfloat16),
-        in_specs=[pl.BlockSpec(memory_space=pltpu.SMEM)] + [vmem] * (blocks + 1),
-        out_specs=vmem,
+        in_specs=[SMEM] + [VMEM] * (blocks + 1),
+        out_specs=VMEM,
         name="gate_and_up",
-        compiler_params=pltpu.CompilerParams(vmem_limit_bytes=16 * 2**20),
+        compiler_params=LIMIT,
         cost_estimate=pl.CostEstimate(
             flops=2 * blocks * units * block * rows, bytes_accessed=2 * blocks * units * block, transcendentals=0
         ),
@@ -133,46 +207,22 @@
 
     tok = tokens.T
     gathered = lax.all_gather(tok, "tp", axis=0, tiled=True)
-    wide_tok = gathered.astype(f32)
-    squares = jnp.sum(wide_tok * wide_tok, axis=0)
-    gain = norm_attn.astype(f32)[:, None]
-    parts = jnp.concatenate(
-        [
-            lax.dot_general(
-                gathered,
-                (w.astype(f32) * gain).astype(bf16),
-                (((0,), (0,)), ((), ())),
-                preferred_element_type=f32,
-            )
-            for w in (w_query, w_key, w_value, w_gate)
-        ],
-        axis=1,
-    ).astype(bf16)
-    terms = jnp.stack([t.reshape(n_kv, own) for t in in_three(squares)], axis=1)
-    terms = jnp.pad(terms, ((0, 0), (0, 1), (0, parts.shape[1] - own)))
-    sent = jnp.concatenate([parts.reshape(n_kv, own, -1), terms], axis=1)
+    sent = project(gathered, norm_attn[None], (w_query, w_key, w_value, w_gate), n_kv)
     got = lax.all_to_all(sent, "kv", 0, 0, tiled=True)
-    summed = jnp.sum(got.astype(f32), axis=0)
-    own_squares = summed[own, :own] + summed[own + 1, :own] + summed[own + 2, :own]
-    projected = summed[:own] * lax.rsqrt(own_squares / D + epsilon)[:, None]
 
     half = head_size // 2
     inverse = 10000.0 ** (-jnp.arange(half, dtype=f32) / half)
     angles = lengths.astype(f32)[:, None] * inverse[None, :]
-    cosine, sine = jnp.cos(angles)[:, None, :], jnp.sin(angles)[:, None, :]
-    heads = [
-        projected[:, i * width : (i + 1) * width].reshape(own, heads_local, head_size)
-        for i in range(3)
-    ]
+    cosine, sine = jnp.cos(angles), jnp.sin(angles)
+    cosine = jnp.concatenate([cosine, cosine], axis=1)
+    sine = jnp.concatenate([-sine, sine], axis=1)
     decay_rate = head_decay(lax.axis_index("tp") * heads_local + jnp.arange(heads_local))
-    new_memory, mixed = retain(
-        memory,
-        rotate(heads[0], cosine, sine),
-        rotate(heads[1], cosine, sine),
-        heads[2],
-        projected[:, 3 * width :],
-        head_gain,
-        decay_rate,
+    start = (lax.axis_index("kv") * own)[None]
+    mixed, keys, values = attend(
+        decay_rate, start, got, cosine, sine, memory[:, 0], head_gain[None], rows
+    )
+    new_memory = (
+        decay_rate[None, :, None, None] * memory + (keys[:, :, None] * values[:, None, :])[:, None]
     )
 
     four = 4
@@ -191,7 +241,7 @@
         lax.ppermute(wide[j], "kv", [(k, k ^ j) for k in range(n_kv)]) for j in range(1, four)
     ]
 
-    mixed_all = from_everyone(mixed, "kv").reshape(rows, width)
+    mixed_all = lax.all_to_all(mixed, "kv", 0, 0, tiled=True).reshape(rows, width)
     attn_part = lax.dot_general(
         w_out, mixed_all, (((0,), (1,)), ((), ())), preferred_element_type=f32
     ).astype(bf16)

time: 241 us -> 243 us (level)
  blocking collectives: 149 us -> 126 us
  starting transfers between devices: 37.9 us -> 50.5 us
  waiting for transfers between devices: 31.4 us -> 40.3 us
  local copies, waits for them, and re-layouts: 3.78 us -> 8.33 us
  matrix products: 4.64 us -> 0.59 us
  Pallas kernels: 1.27 us -> 5.07 us
    all_to_all x1 -> x0, blocking collectives: 22.5 us -> none  [per_device(): down = lax.all_to_all(down.reshape(n_tp, -1, rows), 'tp', 0, 0, tiled=True)]
    all_to_all x1 -> x2, starting transfers between devices: 11.1 us -> 23.6 us  [the longest x1 12.3 us: per_device(): down = lax.all_to_all(down.reshape(n_tp, -1, rows), 'tp', 0, 0, tiled=True)]
    all_to_all x1 -> x2, waiting for transfers between devices: 5.34 us -> 14.4 us  [the longest x1 8.73 us: per_device(): down = lax.all_to_all(down.reshape(n_tp, -1, rows), 'tp', 0, 0, tiled=True)]
    dot_general x5 -> x0, matrix products: 4.06 us -> none  [the longest x4 2.86 us: per_device(): lax.dot_general(gathered, (w.astype(f32) * gain).astype(bf16), (((0,), (0...]
    pallas_call x0 -> x2, Pallas kernels: none -> 3.81 us  [the longest x1 2.24 us: project(): pl.pallas_call(kernel, out_shape=jax.ShapeDtypeStruct((pieces, height, co...]
    unnamed x26 -> x28, local copies, waits for them, and re-layouts: 0.51 us -> 3.84 us
    all_gather x1, blocking collectives: 30.5 us -> 33.3 us  [per_device(): hidden = lax.all_gather(hidden.astype(bf16), 'kv', axis=0, tiled=True)]
    all_to_all x1, blocking collectives: 22 us -> 19.4 us  [per_device(): both = lax.all_to_all(both, 'kv', 0, 0, axis_index_groups=far, tiled=True)]
  transfers between devices with their start and end apart: 7 -> 8, of which waited for: 3 -> 4; matrix products, arithmetic and copies ran while one was open for 1% -> 2% of each run, Pallas kernels for 0% -> 0%
where the time goes in v4:
time: 243 us; the launch traced here: 242 us
  blocking collectives  126 us (52%)
  starting transfers between devices  50.5 us (21%)
  waiting for transfers between devices  40.3 us (17%)
  between operations  8.35 us (3%)
  local copies, waits for them, and re-layouts  8.33 us (3%)
  Pallas kernels  5.07 us (2%)
  other arithmetic  2.92 us (1%)
    all_gather x1, blocking collectives, per_device(): gathered = lax.all_gather(tok, 'tp', axis=0, tiled=True)  56.3 us
    all_gather x1, blocking collectives, per_device(): hidden = lax.all_gather(hidden.astype(bf16), 'kv', axis=0, tiled=True)  33.3 us
    all_to_all x1, blocking collectives, per_device(): both = lax.all_to_all(both, 'kv', 0, 0, axis_index_groups=far, tiled=True)  19.4 us
    all_to_all x1, waiting for transfers between devices, per_device(): got = lax.all_to_all(sent, 'kv', 0, 0, tiled=True)  18.6 us
    all_gather x1, blocking collectives, per_device(): mid_all = lax.all_gather(mid_near, 'tp', axis=1, tiled=True)  17.4 us
    all_to_all x1, starting transfers between devices, per_device(): down = lax.all_to_all(down.reshape(n_tp, -1, rows), 'tp', 0, 0, tiled=True)  12.3 us
    all_to_all x1, starting transfers between devices, per_device(): lax.all_to_all(mixed, 'kv', 0, 0, tiled=True).reshape(rows, width)  11.2 us
    ppermute x3, starting transfers between devices, per_device(): lax.ppermute(wide[j], 'kv', [(k, k ^ j) for k in range(n_kv)])  9.35 us
  transfers between devices with their start and end apart: 8, of which 4 were waited for; matrix products, arithmetic and copies ran while one was open for 2% of the time, Pallas kernels for 0%

profile of v4, /device:TPU:65, one launch (start us, length us, event | category | flops | bytes accessed | tf_op | source)
XLA Modules:
  0.0 242.4 jit_solution(11347172577823045661)
XLA Ops:
  0.7 0.8 broadcast_in_dim.9.norm_ref
  1.4 56.3 %all_gather.9.tokens_ref = bf16[256,320]{1,0:T(8,128)(2,1)S(1)} all-gather(bf16[16,320]{1,0:T(8,128)(2,1)} %bitcast.52), channel_id=1, replica_groups=mesh['grp'=2,'kv'=16,'tp'=16] {'tp'}, dimensions={0}, use_global_device_ids=true | all-gather | bytes 174080 | tf_op jit(solution)/shard_map/all_gather | solution.py:209
  57.7 0.8 copy-done.2
  58.6 0.8 copy-done.3
  59.4 0.8 copy-done.4
  60.3 0.8 copy-done.5
  61.1 2.2 project.1
  63.4 7.2 %all-to-all-start = ((bf16[16,24,512]{2,1,0:T(8,128)(2,1)}), bf16[16,24,512]{2,1,0:T(8,128)(2,1)S(1)}, u32[]{:S(2)}, u32[]{:S(2)}) async-start(bf16[16,24,512]{2,1,0:T(8,128)(2,1)} %project.1), calls=%async_computation | async-start | bytes 786432 | tf_op jit(solution)/shard_map/all_to_all | solution.py:211
  70.9 18.6 %all-to-all-done.parts_ref = bf16[16,24,512]{2,1,0:T(8,128)(2,1)S(1)} async-done(((bf16[16,24,512]{2,1,0:T(8,128)(2,1)}), bf16[16,24,512]{2,1,0:T(8,128)(2,1)S(1)}, u32[]{:S(2)}, u32[]{:S(2)}) %all-to-all-start) | async-done | bytes 393248 | tf_op jit(solution)/shard_map/all_to_all | solution.py:211
  89.5 1.6 attend.1
  91.1 11.2 %all-to-all-start.1 = ((bf16[16,20,128]{2,1,0:T(8,128)(2,1)}), bf16[16,20,128]{2,1,0:T(8,128)(2,1)S(1)}, u32[]{:S(2)}, u32[]{:S(2)}) async-start(bf16[16,20,128]{2,1,0:T(8,128)(2,1)} %get-tuple-element.5), calls=%async_computation.1 | async-start | bytes 196608 | tf_op jit(solution)/shard_map/all_to_all | solution.py:244
  102.3 0.6 fusion.8
  108.3 5.6 %all-to-all-done.1 = bf16[16,20,128]{2,1,0:T(8,128)(2,1)S(1)} async-done(((bf16[16,20,128]{2,1,0:T(8,128)(2,1)}), bf16[16,20,128]{2,1,0:T(8,128)(2,1)S(1)}, u32[]{:S(2)}, u32[]{:S(2)}) %all-to-all-start.1) | async-done | bytes 81952 | tf_op jit(solution)/shard_map/all_to_all | solution.py:244
  114.2 0.8 copy.21
  115.0 7.0 %all-to-all-start.2 = ((bf16[16,16,320]{2,1,0:T(8,128)(2,1)}), bf16[16,16,320]{2,1,0:T(8,128)(2,1)S(1)}, u32[]{:S(2)}, u32[]{:S(2)}) async-start(bf16[16,16,320]{2,1,0:T(8,128)(2,1)} %bitcast.6), calls=%async_computation.2 | async-start | bytes 393216 | tf_op jit(solution)/shard_map/all_to_all | solution.py:248
  124.9 7.3 %all-to-all-done.2 = bf16[16,16,320]{2,1,0:T(8,128)(2,1)S(1)} async-done(((bf16[16,16,320]{2,1,0:T(8,128)(2,1)}), bf16[16,16,320]{2,1,0:T(8,128)(2,1)S(1)}, u32[]{:S(2)}, u32[]{:S(2)}) %all-to-all-start.2) | async-done | bytes 163872 | tf_op jit(solution)/shard_map/all_to_all | solution.py:248
  132.3 0.6 broadcast_in_dim.11
  132.9 3.4 %all-to-all-start.3 = ((bf16[4,16,320]{2,1,0:T(8,128)(2,1)}), bf16[4,16,320]{2,1,0:T(8,128)(2,1)S(1)}, u32[]{:S(2)}, u32[]{:S(2)}) async-start(bf16[4,16,320]{2,1,0:T(8,128)(2,1)} %broadcast_in_dim.11), calls=%async_computation.3 | async-start | bytes 98304 | tf_op jit(solution)/shard_map/all_to_all | solution.py:252
  136.2 0.8 dynamic-slice_bitcast_fusion
  137.0 5.1 %collective-permute-start.2 = (bf16[448,256]{1,0:T(8,128)(2,1)}, bf16[448,256]{1,0:T(8,128)(2,1)S(1)}, u32[]{:S(2)}, u32[]{:S(2)}) collective-permute-start(bf16[448,256]{1,0:T(8,128)(2,1)} %get-tuple-element.8), channel_id=1, source_target_pairs={{0,48},{16,32},{32,16},{48,0},{64,112},{80,96},{96,80},{112,64},{1... | collective-permute-start | bytes 688136 | tf_op jit(solution)/shard_map/ppermute | solution.py:241
  142.1 2.0 collective-permute-start.1
  144.1 2.3 collective-permute-start
  146.4 17.4 %all_gather.10.refs_4_ = bf16[4,256,320]{2,1,0:T(8,128)(2,1)S(1)} all-gather(bf16[4,16,320]{2,1,0:T(8,128)(2,1)S(1)} %all-to-all-done.3), channel_id=1, replica_groups=mesh['grp'=2,'kv'=16,'tp'=16] {'tp'}, dimensions={1}, use_global_device_ids=true | all-gather | bytes 696320 | tf_op jit(solution)/shard_map/all_gather | solution.py:253
  163.8 1.3 gate_and_up.1
  165.1 19.4 %all_to_all.30 = bf16[4,64,640]{2,1,0:T(8,128)(2,1)S(1)} all-to-all(bf16[4,64,640]{2,1,0:T(8,128)(2,1)S(1)} %gate_and_up.1), channel_id=1, replica_groups={{0,64,128,192},{16,80,144,208},{32,96,160,224},{48,112,176,240},{1,65,1..., dimensions={0} | all-to-all | bytes 655360 | tf_op jit(solution)/shard_map/all_to_all | solution.py:255
  184.7 33.3 %all_gather.11 = bf16[896,320]{1,0:T(8,128)(2,1)S(1)} all-gather(bf16[56,320]{1,0:T(8,128)(2,1)S(1)} %fusion.3), channel_id=1, replica_groups=mesh['grp'=2,'kv'=16,'tp'=16] {'kv'}, dimensions={0}, use_global_device_ids=true | all-gather | bytes 609280 | tf_op jit(solution)/shard_map/all_gather | solution.py:260
  218.0 0.4 fusion
  218.4 0.8 copy.25
  219.2 12.3 %all-to-all-start.5 = ((bf16[16,16,320]{2,1,0:T(8,128)(2,1)}), bf16[16,16,320]{2,1,0:T(8,128)(2,1)S(1)}, u32[]{:S(2)}, u32[]{:S(2)}) async-start(bf16[16,16,320]{2,1,0:T(8,128)(2,1)} %bitcast.23), calls=%async_computation.5 | async-start | bytes 393216 | tf_op jit(solution)/shard_map/all_to_all | solution.py:264
  231.5 1.5 multiply_add_fusion
  233.0 8.7 %all-to-all-done.5 = bf16[16,16,320]{2,1,0:T(8,128)(2,1)S(1)} async-done(((bf16[16,16,320]{2,1,0:T(8,128)(2,1)}), bf16[16,16,320]{2,1,0:T(8,128)(2,1)S(1)}, u32[]{:S(2)}, u32[]{:S(2)}) %all-to-all-start.5) | async-done | bytes 163872 | tf_op jit(solution)/shard_map/all_to_all | solution.py:264
  241.8 0.6 fusion.4
  (45 shorter events, 1.6 us)
Async XLA Ops:
  0.6 217.4 %copy-start = (bf16[896,256]{1,0:T(8,128)(2,1)S(1)}, bf16[896,256]{1,0:T(8,128)(2,1)}, u32[]{:S(2)}) copy-start(bf16[896,256]{1,0:T(8,128)(2,1)} %param.27) | copy-start | bytes 1376260
  0.6 88.8 %copy-start.1 = (f32[20,1,128,128]{3,2,1,0:T(8,128)S(1)}, f32[20,1,128,128]{3,2,1,0:T(8,128)}, u32[]{:S(2)}) copy-start(f32[20,1,128,128]{3,2,1,0:T(8,128)} %param.16) | copy-start | bytes 3932164
  57.7 0.8 copy-start.2
  58.6 0.8 copy-start.3
  59.4 0.8 copy-start.4
  60.3 0.8 copy-start.5
  61.1 9.6 %copy-start.11 = (s32[20]{0:T(128)S(1)}, s32[20]{0:T(128)}, u32[]{:S(2)}) copy-start(s32[20]{0:T(128)} %param.15) | copy-start | bytes 244
  61.1 28.4 %copy-start.6 = (bf16[128]{0:T(256)(128)(2,1)S(1)}, bf16[128]{0:T(256)(128)(2,1)}, u32[]{:S(2)}) copy-start(bf16[128]{0:T(256)(128)(2,1)} %param.22) | copy-start | bytes 772
  63.4 44.5 %copy-start.12 = (bf16[256]{0:T(256)(128)(2,1)S(1)}, bf16[256]{0:T(256)(128)(2,1)}, u32[]{:S(2)}) copy-start(bf16[256]{0:T(256)(128)(2,1)} %param.24) | copy-start | bytes 1540
  63.4 44.5 %copy-start.7 = (bf16[256,896]{1,0:T(8,128)(2,1)S(1)}, bf16[256,896]{1,0:T(8,128)(2,1)}, u32[]{:S(2)}) copy-start(bf16[256,896]{1,0:T(8,128)(2,1)} %param.25) | copy-start | bytes 1376260
  63.4 26.1 %all-to-all-start = ((bf16[16,24,512]{2,1,0:T(8,128)(2,1)}), bf16[16,24,512]{2,1,0:T(8,128)(2,1)S(1)}, u32[]{:S(2)}, u32[]{:S(2)}) async-start(bf16[16,24,512]{2,1,0:T(8,128)(2,1)} %project.1), calls=%async_computation | async-start | bytes 786432 | tf_op jit(solution)/shard_map/all_to_all | solution.py:211
  89.5 18.6 %copy-start.8 = (bf16[256,896]{1,0:T(8,128)(2,1)S(1)}, bf16[256,896]{1,0:T(8,128)(2,1)}, u32[]{:S(2)}) copy-start(bf16[256,896]{1,0:T(8,128)(2,1)} %param.26) | copy-start | bytes 1376260
  91.1 22.9 %copy-start.10 = (bf16[128,256]{1,0:T(8,128)(2,1)S(1)}, bf16[128,256]{1,0:T(8,128)(2,1)}, u32[]{:S(2)}) copy-start(bf16[128,256]{1,0:T(8,128)(2,1)} %param.23) | copy-start | bytes 196612
  91.1 22.9 %all-to-all-start.1 = ((bf16[16,20,128]{2,1,0:T(8,128)(2,1)}), bf16[16,20,128]{2,1,0:T(8,128)(2,1)S(1)}, u32[]{:S(2)}, u32[]{:S(2)}) async-start(bf16[16,20,128]{2,1,0:T(8,128)(2,1)} %get-tuple-element.5), calls=%async_computation.1 | async-start | bytes 196608 | tf_op jit(solution)/shard_map/all_to_all | solution.py:244
  115.0 17.2 %all-to-all-start.2 = ((bf16[16,16,320]{2,1,0:T(8,128)(2,1)}), bf16[16,16,320]{2,1,0:T(8,128)(2,1)S(1)}, u32[]{:S(2)}, u32[]{:S(2)}) async-start(bf16[16,16,320]{2,1,0:T(8,128)(2,1)} %bitcast.6), calls=%async_computation.2 | async-start | bytes 393216 | tf_op jit(solution)/shard_map/all_to_all | solution.py:248
  122.3 9.9 %copy-start.9 = (bf16[320,16]{0,1:T(8,128)(2,1)S(1)}, bf16[320,16]{0,1:T(8,128)(2,1)}, u32[]{:S(2)}) copy-start(bf16[320,16]{0,1:T(8,128)(2,1)} %param.14) | copy-start | bytes 30724
  132.9 13.5 %all-to-all-start.3 = ((bf16[4,16,320]{2,1,0:T(8,128)(2,1)}), bf16[4,16,320]{2,1,0:T(8,128)(2,1)S(1)}, u32[]{:S(2)}, u32[]{:S(2)}) async-start(bf16[4,16,320]{2,1,0:T(8,128)(2,1)} %broadcast_in_dim.11), calls=%async_computation.3 | async-start | bytes 98304 | tf_op jit(solution)/shard_map/all_to_all | solution.py:252
  137.0 26.8 %collective-permute-start.2 = (bf16[448,256]{1,0:T(8,128)(2,1)}, bf16[448,256]{1,0:T(8,128)(2,1)S(1)}, u32[]{:S(2)}, u32[]{:S(2)}) collective-permute-start(bf16[448,256]{1,0:T(8,128)(2,1)} %get-tuple-element.8), channel_id=1, source_target_pairs={{0,48},{16,32},{32,16},{48,0},{64,112},{80,96},{96,80},{112,64},{1... | collective-permute-start | bytes 688136 | tf_op jit(solution)/shard_map/ppermute | solution.py:241
  142.1 21.7 %collective-permute-start.1 = (bf16[448,256]{1,0:T(8,128)(2,1)S(1)}, bf16[448,256]{1,0:T(8,128)(2,1)S(1)}, u32[]{:S(2)}, u32[]{:S(2)}) collective-permute-start(bf16[448,256]{1,0:T(8,128)(2,1)S(1)} %get-tuple-element.9), channel_id=1, source_target_pairs={{0,32},{16,48},{32,0},{48,16},{64,96},{80,112},{96,64},{112,80},{1... | collective-permute-start | bytes 688136 | tf_op jit(solution)/shard_map/ppermute | solution.py:241
  144.1 19.7 %collective-permute-start = (bf16[448,256]{1,0:T(8,128)(2,1)S(1)}, bf16[448,256]{1,0:T(8,128)(2,1)S(1)}, u32[]{:S(2)}, u32[]{:S(2)}) collective-permute-start(bf16[448,256]{1,0:T(8,128)(2,1)S(1)} %get-tuple-element.10), channel_id=1, source_target_pairs={{0,16},{16,0},{32,48},{48,32},{64,80},{80,64},{96,112},{112,96},{1... | collective-permute-start | bytes 688136 | tf_op jit(solution)/shard_map/ppermute | solution.py:241
  219.2 22.5 %all-to-all-start.5 = ((bf16[16,16,320]{2,1,0:T(8,128)(2,1)}), bf16[16,16,320]{2,1,0:T(8,128)(2,1)S(1)}, u32[]{:S(2)}, u32[]{:S(2)}) async-start(bf16[16,16,320]{2,1,0:T(8,128)(2,1)} %bitcast.23), calls=%async_computation.5 | async-start | bytes 393216 | tf_op jit(solution)/shard_map/all_to_all | solution.py:264

commit v5 on v4

--- a/solution.py
+++ b/solution.py
@@ -31,73 +31,67 @@
 LIMIT = pltpu.CompilerParams(vmem_limit_bytes=16 * 2**20)
 
 
-def project(gathered, norm, weights, pieces):
+def project(gathered, weights, pieces):
     block, rows = gathered.shape
-    width = weights[0].shape[1]
-    count = len(weights)
+    count, _, width = weights.shape
     own = rows // pieces
-    height = -(-(own + 3) // 8) * 8
-
-    def kernel(tokens_ref, norm_ref, *refs):
-        out_ref, held_ref, arrived = refs[count:]
-        copies = [
-            pltpu.make_async_copy(refs[c], held_ref.at[c], arrived.at[c]) for c in range(count)
+    lines = -(-rows // width)
+    height = -(-(count * own + 2 * lines) // 8) * 8
+
+    def kernel(tokens_ref, weights_ref, out_ref):
+        held = tokens_ref[...]
+        value = held.astype(jnp.float32)
+        squares = jnp.sum(value * value, axis=0, keepdims=True)
+        squares = jnp.concatenate(
+            [squares, jnp.zeros((1, lines * width - rows), jnp.float32)], axis=1
+        )
+        terms = [term.astype(jnp.float32) for term in in_three(squares)[:2]]
+        under = jnp.concatenate(
+            [term[:, i * width : (i + 1) * width] for term in terms for i in range(lines)]
+            + [jnp.zeros((height - count * own - 2 * lines, width), jnp.float32)],
+            axis=0,
+        )
+        products = [
+            lax.dot_general(
+                held, weights_ref[c], (((0,), (0,)), ((), ())), preferred_element_type=jnp.float32
+            )
+            for c in range(count)
         ]
-        for copy in copies:
-            copy.start()
-        value = tokens_ref[...].astype(jnp.float32)
-        squares = jnp.sum(value * value, axis=0, keepdims=True)
-        gain = jnp.broadcast_to(norm_ref[...].astype(jnp.float32), (128, block)).T[:, :1]
-        scaled = (value * gain).astype(jnp.bfloat16)
-        under = [term.astype(jnp.float32) for term in in_three(squares)]
-        under = jnp.concatenate(under + [jnp.zeros((height - own - 3, rows), jnp.float32)], axis=0)
-        under = jnp.concatenate(
-            [under, jnp.zeros((height - own, count * width - rows), jnp.float32)], axis=1
-        )
-        for c in range(count):
-            copies[c].wait()
-            product = lax.dot_general(
-                scaled, held_ref[c], (((0,), (0,)), ((), ())), preferred_element_type=jnp.float32
-            )
-            span = slice(c * width, (c + 1) * width)
-            for p in range(pieces):
-                piece = jnp.concatenate([product[p * own : (p + 1) * own], under[:, span]], axis=0)
-                out_ref[p, :, span] = piece.astype(jnp.bfloat16)
+        for p in range(pieces):
+            piece = [product[p * own : (p + 1) * own] for product in products]
+            out_ref[p] = jnp.concatenate(piece + [under], axis=0).astype(jnp.bfloat16)
 
     return pl.pallas_call(
         kernel,
-        out_shape=jax.ShapeDtypeStruct((pieces, height, count * width), jnp.bfloat16),
-        in_specs=[VMEM] * 2 + [pl.BlockSpec(memory_space=pl.ANY)] * count,
+        out_shape=jax.ShapeDtypeStruct((pieces, height, width), jnp.bfloat16),
+        in_specs=[VMEM] * 2,
         out_specs=VMEM,
-        scratch_shapes=[
-            pltpu.VMEM((count, block, width), jnp.bfloat16),
-            pltpu.SemaphoreType.DMA((count,)),
-        ],
         name="project",
         compiler_params=LIMIT,
         cost_estimate=pl.CostEstimate(
             flops=2 * count * block * width * rows, bytes_accessed=2 * gathered.size, transcendentals=0
         ),
-    )(gathered, norm, *weights)
+    )(gathered, weights)
 
 
 def attend(scalars, start, parts, cosine, sine, memory, head_gain, rows):
-    pieces, _, _ = parts.shape
+    pieces = parts.shape[0]
     own, size, _ = memory.shape
+    lines = -(-rows // size)
 
     def kernel(scalars_ref, start_ref, parts_ref, cos_ref, sin_ref, memory_ref, gain_ref, *refs):
         mixed_ref, keys_ref, values_ref, read_ref = refs
         summed = parts_ref[0].astype(jnp.float32)
         for p in range(1, pieces):
             summed = summed + parts_ref[p].astype(jnp.float32)
-        total = summed[own : own + 1, :rows] + summed[own + 1 : own + 2, :rows]
-        total = total + summed[own + 2 : own + 3, :rows]
-        lane = lax.broadcasted_iota(jnp.int32, (own, rows), 1)
-        line = lax.broadcasted_iota(jnp.int32, (own, rows), 0) + start_ref[0]
+        total = summed[4 * own : 4 * own + lines] + summed[4 * own + lines : 4 * own + 2 * lines]
+        total = jnp.concatenate([total[i : i + 1] for i in range(lines)], axis=1)
+        lane = lax.broadcasted_iota(jnp.int32, (own, lines * size), 1)
+        line = lax.broadcasted_iota(jnp.int32, (own, lines * size), 0) + start_ref[0]
         total = jnp.sum(jnp.where(lane == line, total, 0.0), axis=1, keepdims=True)
         scale = lax.rsqrt(total / D + epsilon)
         query, key, value, gate = (
-            summed[:own, i * size : (i + 1) * size] * scale for i in range(4)
+            summed[i * own : (i + 1) * own] * scale for i in range(4)
         )
         query, key = (
             x * cos_ref[...] + pltpu.roll(x, size // 2, 1) * sin_ref[...] for x in (query, key)
@@ -206,8 +200,13 @@
     ff = w_up.shape[1]
 
     tok = tokens.T
-    gathered = lax.all_gather(tok, "tp", axis=0, tiled=True)
-    sent = project(gathered, norm_attn[None], (w_query, w_key, w_value, w_gate), n_kv)
+    gathered = jnp.broadcast_to(tok, (n_tp, *tok.shape))
+    gathered = lax.all_to_all(gathered, "tp", 0, 0, tiled=True).reshape(block, rows)
+    gain = norm_attn.astype(f32)[:, None]
+    folded = jnp.stack(
+        [(w.astype(f32) * gain).astype(bf16) for w in (w_query, w_key, w_value, w_gate)]
+    )
+    sent = project(gathered, folded, n_kv)
     got = lax.all_to_all(sent, "kv", 0, 0, tiled=True)
 
     half = head_size // 2

time: 243 us -> 236 us (0.971)
  blocking collectives: 126 us -> 69.8 us
  starting transfers between devices: 50.5 us -> 92.8 us
  waiting for transfers between devices: 40.3 us -> 49 us
  local copies, waits for them, and re-layouts: 8.33 us -> 5.7 us
    all_gather x1 -> x0, blocking collectives: 56.3 us -> none  [per_device(): gathered = lax.all_gather(tok, 'tp', axis=0, tiled=True)]
    all_to_all x0 -> x1, starting transfers between devices: none -> 44.8 us  [per_device(): lax.all_to_all(gathered, 'tp', 0, 0, tiled=True).reshape(block, rows)]
    all_to_all x0 -> x1, waiting for transfers between devices: none -> 8.78 us  [per_device(): lax.all_to_all(gathered, 'tp', 0, 0, tiled=True).reshape(block, rows)]
    unnamed x28 -> x20, local copies, waits for them, and re-layouts: 3.84 us -> 0.48 us
  transfers between devices with their start and end apart: 8 -> 9, of which waited for: 4 -> 5; matrix products, arithmetic and copies ran while one was open for 2% -> 2% of each run, Pallas kernels for 0% -> 0%
where the time goes in v5:
time: 236 us; the launch traced here: 235 us
  starting transfers between devices  92.8 us (39%)
  blocking collectives  69.8 us (30%)
  waiting for transfers between devices  49 us (21%)
  between operations  8.52 us (4%)
  local copies, waits for them, and re-layouts  5.7 us (2%)
  other arithmetic  4.77 us (2%)
  Pallas kernels  3.93 us (2%)
    all_to_all x1, starting transfers between devices, per_device(): lax.all_to_all(gathered, 'tp', 0, 0, tiled=True).reshape(block, rows)  44.8 us
    all_gather x1, blocking collectives, per_device(): hidden = lax.all_gather(hidden.astype(bf16), 'kv', axis=0, tiled=True)  31.6 us
    all_to_all x1, blocking collectives, per_device(): both = lax.all_to_all(both, 'kv', 0, 0, axis_index_groups=far, tiled=True)  21.2 us
    all_to_all x1, waiting for transfers between devices, per_device(): got = lax.all_to_all(sent, 'kv', 0, 0, tiled=True)  18.2 us
    all_gather x1, blocking collectives, per_device(): mid_all = lax.all_gather(mid_near, 'tp', axis=1, tiled=True)  16.9 us
    all_to_all x1, starting transfers between devices, per_device(): down = lax.all_to_all(down.reshape(n_tp, -1, rows), 'tp', 0, 0, tiled=True)  12.1 us
    all_to_all x1, starting transfers between devices, per_device(): lax.all_to_all(mixed, 'kv', 0, 0, tiled=True).reshape(rows, width)  10.2 us
    ppermute x3, starting transfers between devices, per_device(): lax.ppermute(wide[j], 'kv', [(k, k ^ j) for k in range(n_kv)])  9.35 us
  transfers between devices with their start and end apart: 9, of which 5 were waited for; matrix products, arithmetic and copies ran while one was open for 2% of the time, Pallas kernels for 0%

profile of v5, /device:TPU:65, one launch (start us, length us, event | category | flops | bytes accessed | tf_op | source)
XLA Modules:
  0.0 235.1 jit_solution(6937037964391054583)
XLA Ops:
  0.6 1.5 broadcast_in_dim.9
  2.1 44.8 %all-to-all-start = ((bf16[16,16,320]{2,1,0:T(8,128)(2,1)}), bf16[16,16,320]{2,1,0:T(8,128)(2,1)S(1)}, u32[]{:S(2)}, u32[]{:S(2)}) async-start(bf16[16,16,320]{2,1,0:T(8,128)(2,1)} %broadcast_in_dim.9), calls=%async_computation | async-start | bytes 393216 | tf_op jit(solution)/shard_map/all_to_all | solution.py:204
  46.9 0.7 convert_element_type.96
  47.5 1.2 fusion.4
  48.7 8.8 %all-to-all-done = bf16[16,16,320]{2,1,0:T(8,128)(2,1)S(1)} async-done(((bf16[16,16,320]{2,1,0:T(8,128)(2,1)}), bf16[16,16,320]{2,1,0:T(8,128)(2,1)S(1)}, u32[]{:S(2)}, u32[]{:S(2)}) %all-to-all-start) | async-done | bytes 163872 | tf_op jit(solution)/shard_map/all_to_all | solution.py:204
  57.5 1.1 project.1
  58.6 7.1 %all-to-all-start.1 = ((bf16[16,88,128]{2,1,0:T(8,128)(2,1)}), bf16[16,88,128]{2,1,0:T(8,128)(2,1)S(1)}, u32[]{:S(2)}, u32[]{:S(2)}) async-start(bf16[16,88,128]{2,1,0:T(8,128)(2,1)} %project.1), calls=%async_computation.1 | async-start | bytes 720896 | tf_op jit(solution)/shard_map/all_to_all | solution.py:210
  66.0 18.2 %all-to-all-done.1.parts_ref = bf16[16,88,128]{2,1,0:T(8,128)(2,1)S(1)} async-done(((bf16[16,88,128]{2,1,0:T(8,128)(2,1)}), bf16[16,88,128]{2,1,0:T(8,128)(2,1)S(1)}, u32[]{:S(2)}, u32[]{:S(2)}) %all-to-all-start.1) | async-done | bytes 360480 | tf_op jit(solution)/shard_map/all_to_all | solution.py:210
  84.3 1.6 attend.1
  85.8 10.2 %all-to-all-start.2 = ((bf16[16,20,128]{2,1,0:T(8,128)(2,1)}), bf16[16,20,128]{2,1,0:T(8,128)(2,1)S(1)}, u32[]{:S(2)}, u32[]{:S(2)}) async-start(bf16[16,20,128]{2,1,0:T(8,128)(2,1)} %get-tuple-element.5), calls=%async_computation.2 | async-start | bytes 196608 | tf_op jit(solution)/shard_map/all_to_all | solution.py:243
  96.0 0.7 fusion.12
  101.8 0.2 copy.22
  102.2 5.5 %all-to-all-done.2 = bf16[16,20,128]{2,1,0:T(8,128)(2,1)S(1)} async-done(((bf16[16,20,128]{2,1,0:T(8,128)(2,1)}), bf16[16,20,128]{2,1,0:T(8,128)(2,1)S(1)}, u32[]{:S(2)}, u32[]{:S(2)}) %all-to-all-start.2) | async-done | bytes 81952 | tf_op jit(solution)/shard_map/all_to_all | solution.py:243
  108.0 0.8 copy.21
  108.8 6.0 %all-to-all-start.3 = ((bf16[16,16,320]{2,1,0:T(8,128)(2,1)}), bf16[16,16,320]{2,1,0:T(8,128)(2,1)S(1)}, u32[]{:S(2)}, u32[]{:S(2)}) async-start(bf16[16,16,320]{2,1,0:T(8,128)(2,1)} %bitcast.11), calls=%async_computation.3 | async-start | bytes 393216 | tf_op jit(solution)/shard_map/all_to_all | solution.py:247
  117.7 7.7 %all-to-all-done.3 = bf16[16,16,320]{2,1,0:T(8,128)(2,1)S(1)} async-done(((bf16[16,16,320]{2,1,0:T(8,128)(2,1)}), bf16[16,16,320]{2,1,0:T(8,128)(2,1)S(1)}, u32[]{:S(2)}, u32[]{:S(2)}) %all-to-all-start.3) | async-done | bytes 163872 | tf_op jit(solution)/shard_map/all_to_all | solution.py:247
  125.5 0.6 broadcast_in_dim.11
  126.1 3.4 %all-to-all-start.4 = ((bf16[4,16,320]{2,1,0:T(8,128)(2,1)}), bf16[4,16,320]{2,1,0:T(8,128)(2,1)S(1)}, u32[]{:S(2)}, u32[]{:S(2)}) async-start(bf16[4,16,320]{2,1,0:T(8,128)(2,1)} %broadcast_in_dim.11), calls=%async_computation.4 | async-start | bytes 98304 | tf_op jit(solution)/shard_map/all_to_all | solution.py:251
  129.5 0.8 dynamic-slice_bitcast_fusion
  130.3 5.1 %collective-permute-start.2 = (bf16[448,256]{1,0:T(8,128)(2,1)}, bf16[448,256]{1,0:T(8,128)(2,1)S(1)}, u32[]{:S(2)}, u32[]{:S(2)}) collective-permute-start(bf16[448,256]{1,0:T(8,128)(2,1)} %get-tuple-element.8), channel_id=1, source_target_pairs={{0,48},{16,32},{32,16},{48,0},{64,112},{80,96},{96,80},{112,64},{1... | collective-permute-start | bytes 688136 | tf_op jit(solution)/shard_map/ppermute | solution.py:240
  135.4 2.0 collective-permute-start.1
  137.3 2.3 collective-permute-start
  139.7 16.9 %all_gather.6.refs_4_ = bf16[4,256,320]{2,1,0:T(8,128)(2,1)S(1)} all-gather(bf16[4,16,320]{2,1,0:T(8,128)(2,1)S(1)} %all-to-all-done.4), channel_id=1, replica_groups=mesh['grp'=2,'kv'=16,'tp'=16] {'tp'}, dimensions={1}, use_global_device_ids=true | all-gather | bytes 696320 | tf_op jit(solution)/shard_map/all_gather | solution.py:252
  156.6 1.3 gate_and_up.1
  157.9 21.2 %all_to_all.35 = bf16[4,64,640]{2,1,0:T(8,128)(2,1)S(1)} all-to-all(bf16[4,64,640]{2,1,0:T(8,128)(2,1)S(1)} %gate_and_up.1), channel_id=1, replica_groups={{0,64,128,192},{16,80,144,208},{32,96,160,224},{48,112,176,240},{1,65,1..., dimensions={0} | all-to-all | bytes 655360 | tf_op jit(solution)/shard_map/all_to_all | solution.py:254
  179.4 31.6 %all_gather.7 = bf16[896,320]{1,0:T(8,128)(2,1)S(1)} all-gather(bf16[56,320]{1,0:T(8,128)(2,1)S(1)} %fusion.3), channel_id=1, replica_groups=mesh['grp'=2,'kv'=16,'tp'=16] {'kv'}, dimensions={0}, use_global_device_ids=true | all-gather | bytes 609280 | tf_op jit(solution)/shard_map/all_gather | solution.py:259
  211.0 0.4 fusion
  211.4 0.8 copy.25
  212.2 12.1 %all-to-all-start.6 = ((bf16[16,16,320]{2,1,0:T(8,128)(2,1)}), bf16[16,16,320]{2,1,0:T(8,128)(2,1)S(1)}, u32[]{:S(2)}, u32[]{:S(2)}) async-start(bf16[16,16,320]{2,1,0:T(8,128)(2,1)} %bitcast.28), calls=%async_computation.6 | async-start | bytes 393216 | tf_op jit(solution)/shard_map/all_to_all | solution.py:263
  224.3 1.5 multiply_add_fusion
  225.7 8.7 %all-to-all-done.6 = bf16[16,16,320]{2,1,0:T(8,128)(2,1)S(1)} async-done(((bf16[16,16,320]{2,1,0:T(8,128)(2,1)}), bf16[16,16,320]{2,1,0:T(8,128)(2,1)S(1)}, u32[]{:S(2)}, u32[]{:S(2)}) %all-to-all-start.6) | async-done | bytes 163872 | tf_op jit(solution)/shard_map/all_to_all | solution.py:263
  234.5 0.6 fusion.8
  (41 shorter events, 1.4 us)
Async XLA Ops:
  0.6 210.3 %copy-start = (bf16[896,256]{1,0:T(8,128)(2,1)S(1)}, bf16[896,256]{1,0:T(8,128)(2,1)}, u32[]{:S(2)}) copy-start(bf16[896,256]{1,0:T(8,128)(2,1)} %param.27) | copy-start | bytes 1376260
  2.1 55.4 %all-to-all-start = ((bf16[16,16,320]{2,1,0:T(8,128)(2,1)}), bf16[16,16,320]{2,1,0:T(8,128)(2,1)S(1)}, u32[]{:S(2)}, u32[]{:S(2)}) async-start(bf16[16,16,320]{2,1,0:T(8,128)(2,1)} %broadcast_in_dim.9), calls=%async_computation | async-start | bytes 393216 | tf_op jit(solution)/shard_map/all_to_all | solution.py:204
  47.5 18.2 %copy-start.7 = (s32[20]{0:T(128)S(1)}, s32[20]{0:T(128)}, u32[]{:S(2)}) copy-start(s32[20]{0:T(128)} %param.15) | copy-start | bytes 244
  47.5 36.7 %copy-start.1 = (f32[20,1,128,128]{3,2,1,0:T(8,128)S(1)}, f32[20,1,128,128]{3,2,1,0:T(8,128)}, u32[]{:S(2)}) copy-start(f32[20,1,128,128]{3,2,1,0:T(8,128)} %param.16) | copy-start | bytes 3932164
  47.5 36.7 %copy-start.2 = (bf16[128]{0:T(256)(128)(2,1)S(1)}, bf16[128]{0:T(256)(128)(2,1)}, u32[]{:S(2)}) copy-start(bf16[128]{0:T(256)(128)(2,1)} %param.22) | copy-start | bytes 772
  58.6 43.2 %copy-start.8 = (bf16[256]{0:T(256)(128)(2,1)S(1)}, bf16[256]{0:T(256)(128)(2,1)}, u32[]{:S(2)}) copy-start(bf16[256]{0:T(256)(128)(2,1)} %param.24) | copy-start | bytes 1540
  58.6 43.2 %copy-start.3 = (bf16[256,896]{1,0:T(8,128)(2,1)S(1)}, bf16[256,896]{1,0:T(8,128)(2,1)}, u32[]{:S(2)}) copy-start(bf16[256,896]{1,0:T(8,128)(2,1)} %param.25) | copy-start | bytes 1376260
  58.6 25.6 %all-to-all-start.1 = ((bf16[16,88,128]{2,1,0:T(8,128)(2,1)}), bf16[16,88,128]{2,1,0:T(8,128)(2,1)S(1)}, u32[]{:S(2)}, u32[]{:S(2)}) async-start(bf16[16,88,128]{2,1,0:T(8,128)(2,1)} %project.1), calls=%async_computation.1 | async-start | bytes 720896 | tf_op jit(solution)/shard_map/all_to_all | solution.py:210
  84.3 17.8 %copy-start.4 = (bf16[256,896]{1,0:T(8,128)(2,1)S(1)}, bf16[256,896]{1,0:T(8,128)(2,1)}, u32[]{:S(2)}) copy-start(bf16[256,896]{1,0:T(8,128)(2,1)} %param.26) | copy-start | bytes 1376260
  85.8 22.0 %copy-start.6 = (bf16[128,256]{1,0:T(8,128)(2,1)S(1)}, bf16[128,256]{1,0:T(8,128)(2,1)}, u32[]{:S(2)}) copy-start(bf16[128,256]{1,0:T(8,128)(2,1)} %param.23) | copy-start | bytes 196612
  85.8 21.9 %all-to-all-start.2 = ((bf16[16,20,128]{2,1,0:T(8,128)(2,1)}), bf16[16,20,128]{2,1,0:T(8,128)(2,1)S(1)}, u32[]{:S(2)}, u32[]{:S(2)}) async-start(bf16[16,20,128]{2,1,0:T(8,128)(2,1)} %get-tuple-element.5), calls=%async_computation.2 | async-start | bytes 196608 | tf_op jit(solution)/shard_map/all_to_all | solution.py:243
  108.8 16.7 %all-to-all-start.3 = ((bf16[16,16,320]{2,1,0:T(8,128)(2,1)}), bf16[16,16,320]{2,1,0:T(8,128)(2,1)S(1)}, u32[]{:S(2)}, u32[]{:S(2)}) async-start(bf16[16,16,320]{2,1,0:T(8,128)(2,1)} %bitcast.11), calls=%async_computation.3 | async-start | bytes 393216 | tf_op jit(solution)/shard_map/all_to_all | solution.py:247
  115.1 10.4 %copy-start.5 = (bf16[320,16]{0,1:T(8,128)(2,1)S(1)}, bf16[320,16]{0,1:T(8,128)(2,1)}, u32[]{:S(2)}) copy-start(bf16[320,16]{0,1:T(8,128)(2,1)} %param.14) | copy-start | bytes 30724
  126.1 13.5 %all-to-all-start.4 = ((bf16[4,16,320]{2,1,0:T(8,128)(2,1)}), bf16[4,16,320]{2,1,0:T(8,128)(2,1)S(1)}, u32[]{:S(2)}, u32[]{:S(2)}) async-start(bf16[4,16,320]{2,1,0:T(8,128)(2,1)} %broadcast_in_dim.11), calls=%async_computation.4 | async-start | bytes 98304 | tf_op jit(solution)/shard_map/all_to_all | solution.py:251
  130.3 26.3 %collective-permute-start.2 = (bf16[448,256]{1,0:T(8,128)(2,1)}, bf16[448,256]{1,0:T(8,128)(2,1)S(1)}, u32[]{:S(2)}, u32[]{:S(2)}) collective-permute-start(bf16[448,256]{1,0:T(8,128)(2,1)} %get-tuple-element.8), channel_id=1, source_target_pairs={{0,48},{16,32},{32,16},{48,0},{64,112},{80,96},{96,80},{112,64},{1... | collective-permute-start | bytes 688136 | tf_op jit(solution)/shard_map/ppermute | solution.py:240
  135.4 21.2 %collective-permute-start.1 = (bf16[448,256]{1,0:T(8,128)(2,1)S(1)}, bf16[448,256]{1,0:T(8,128)(2,1)S(1)}, u32[]{:S(2)}, u32[]{:S(2)}) collective-permute-start(bf16[448,256]{1,0:T(8,128)(2,1)S(1)} %get-tuple-element.9), channel_id=1, source_target_pairs={{0,32},{16,48},{32,0},{48,16},{64,96},{80,112},{96,64},{112,80},{1... | collective-permute-start | bytes 688136 | tf_op jit(solution)/shard_map/ppermute | solution.py:240
  137.3 19.3 %collective-permute-start = (bf16[448,256]{1,0:T(8,128)(2,1)S(1)}, bf16[448,256]{1,0:T(8,128)(2,1)S(1)}, u32[]{:S(2)}, u32[]{:S(2)}) collective-permute-start(bf16[448,256]{1,0:T(8,128)(2,1)S(1)} %get-tuple-element.10), channel_id=1, source_target_pairs={{0,16},{16,0},{32,48},{48,32},{64,80},{80,64},{96,112},{112,96},{1... | collective-permute-start | bytes 688136 | tf_op jit(solution)/shard_map/ppermute | solution.py:240
  212.2 22.3 %all-to-all-start.6 = ((bf16[16,16,320]{2,1,0:T(8,128)(2,1)}), bf16[16,16,320]{2,1,0:T(8,128)(2,1)S(1)}, u32[]{:S(2)}, u32[]{:S(2)}) async-start(bf16[16,16,320]{2,1,0:T(8,128)(2,1)} %bitcast.28), calls=%async_computation.6 | async-start | bytes 393216 | tf_op jit(solution)/shard_map/all_to_all | solution.py:263
